TPU v7x, 32 devices: a whole 2x2x4 slice. The times are simulated.
32 devices in a mesh: sp: 4 (over y, x), tp: 8 (over z, core).
Axes of the slice: x: 2, y: 2, z: 4, core: 2. Of those that a mesh axis runs over, the one named last changes fastest.
Arguments:
- latent: bfloat16 [2048, 4096], P(('sp', 'tp')), may hold values from -6 to 6
- context: bfloat16 [512, 4096], P('sp'), may hold values from -6 to 6
- condition: float32 [4096], replicated, may hold values from -6 to 6
- context_condition: float32 [4096], replicated, may hold values from -6 to 6
- modulation: bfloat16 [3, 4096, 4096], P(None, 'sp', 'tp'), may hold values from -0.09375 to 0.09375
- query_weight: bfloat16 [4096, 4096], P(None, 'tp'), as said below
- key_weight: bfloat16 [4096, 4096], P(None, 'tp'), as said below
- value_weight: bfloat16 [4096, 4096], P(None, 'tp'), may hold values from -0.09375 to 0.09375
- lambdas: float32 [16], P('tp'), may hold values from 0.3 to 0.8
- context_lift: float32 [16], P('tp'), may hold values from 1.5 to 3
- head_gain: float32 [256], replicated, may hold values from 0.1 to 1.9
- output_weight: bfloat16 [4096, 4096], P('tp'), may hold values from -0.09375 to 0.09375
Outputs:
- result: bfloat16 [2048, 4096], P(('sp', 'tp'))
Inputs may be any that keep to these rules, and one draw needn't show every extreme that they name: `query_weight`: entries lie within 200 / sqrt(4096) in magnitude. `key_weight`: entries lie within 6 / sqrt(4096) in magnitude.
All inputs are finite; a program needn't handle non-finite values.
Results may differ from a plain program's by a relative error of at most 0.025.
Values may be sent and summed in bfloat16 or wider, within the bound.
A program may use at most 64 MiB of HBM per device.

v0:
```python
import functools

import jax
import jax.numpy as jnp
from jax import lax
from jax.experimental import pallas as pl
from jax.experimental.pallas import tpu as pltpu
from jax.sharding import PartitionSpec as P

GRID_W = 64
ROPE_BASE = 10000.0
EPSILON = 1e-05
LOG2E = 1.4426950408889634
ROWS = 16
VMEM_LIMIT = 62 * 1024 * 1024
MESH = pl.DeviceIdType.MESH


def remote(src, dst, send_sem, recv_sem, **where):
    return pltpu.make_async_remote_copy(
        src_ref=src,
        dst_ref=dst,
        send_sem=send_sem,
        recv_sem=recv_sem,
        device_id=where,
        device_id_type=MESH,
    )


def aligned(start, size, unit):
    return pl.ds(pl.multiple_of(start, unit), size)


def attend_kernel(
    sp_size,
    tp_size,
    latent,
    context,
    condition,
    context_condition,
    modulation,
    query_weight,
    key_weight,
    value_weight,
    cosine,
    sine,
    lambdas,
    lift,
    gain,
    attended,
    gate,
    tokens,
    context_tokens,
    normed,
    mod_weight,
    wq,
    wk,
    wv,
    keys_values,
    queries,
    kv_stage,
    q_stage,
    out_stage,
    mod_parts,
    mod_pieces,
    mod_rows,
    local_sem,
    tok_send,
    tok_recv,
    part_send,
    part_recv,
    piece_send,
    piece_recv,
    kv_send,
    kv_recv,
    q_send,
    q_recv,
    out_send,
    out_recv,
):
    s = lax.axis_index("sp")
    t = lax.axis_index("tp")
    z = lax.div(t, 2)
    c = lax.rem(t, 2)
    chips = tp_size // 2
    rows, width = latent.shape
    pair = 2 * rows
    block_tokens = tp_size * rows
    ctx_rows = context.shape[0]
    ctx_total = ctx_rows * sp_size
    local = query_weight.shape[1]
    heads = lambdas.shape[0]
    head = local // heads
    half = head // 2
    piece = modulation.shape[2]
    depth = modulation.shape[1]

    own_slot = tokens.at[aligned(t * rows, rows, ROWS)]
    locals_ = [
        pltpu.make_async_copy(src, dst, local_sem.at[i])
        for i, (src, dst) in enumerate(
            [
                (modulation, mod_weight),
                (latent, own_slot),
                (context, context_tokens),
                (key_weight, wk),
                (value_weight, wv),
                (query_weight, wq),
            ]
        )
    ]
    for copy in locals_:
        copy.start()

    barrier = pltpu.get_barrier_semaphore()
    for k in range(1, tp_size):
        pl.semaphore_signal(
            barrier, inc=1, device_id={"tp": lax.rem(t + k, tp_size)}, device_id_type=MESH
        )
    for k in range(1, sp_size):
        pl.semaphore_signal(
            barrier, inc=1, device_id={"sp": lax.rem(s + k, sp_size)}, device_id_type=MESH
        )
    pl.semaphore_wait(barrier, tp_size + sp_size - 2)

    part_rows = rows // 2

    def token_copy(kind, b, core, part, own=False):
        slot = 2 * b + core
        place = tokens.at[aligned(slot * rows + part * part_rows, part_rows, ROWS)]
        to = (t + 2, t - 2, t + 1 - 2 * c)[kind]
        return remote(
            latent.at[part * part_rows : (part + 1) * part_rows] if own else place,
            place,
            tok_send.at[kind, 2 * b + part],
            tok_recv.at[2 * slot + part],
            tp=to,
        )

    for part in range(2):

        @pl.when(z + 1 < chips)
        def _():
            token_copy(0, z, c, part, True).start()

        @pl.when(z > 0)
        def _():
            token_copy(1, z, c, part, True).start()

        token_copy(2, z, c, part, True).start()

    def silu(ref):
        v = ref[:, aligned(s * depth, depth, 128)]
        return v / (1.0 + jnp.exp(-v))

    first = silu(condition)
    second = silu(context_condition)
    which = lax.broadcasted_iota(jnp.int32, (ROWS, depth), 0)
    vectors = jnp.where(
        which == 0, jnp.broadcast_to(first, (ROWS, depth)), jnp.broadcast_to(second, (ROWS, depth))
    ).astype(jnp.bfloat16)
    locals_[0].wait()
    for r in range(3):
        found = jnp.dot(vectors, mod_weight[r], preferred_element_type=jnp.float32)
        mod_parts[s, 2 * r : 2 * r + 2, :] = found[0:2]
    mod_parts[s, 6:8, :] = jnp.zeros((2, piece), jnp.float32)

    def part_copy(k, owner):
        return remote(
            mod_parts.at[owner],
            mod_parts.at[owner],
            part_send.at[k],
            part_recv.at[owner],
            sp=lax.rem(s + k, sp_size),
        )

    def piece_copy(k, owner):
        return remote(
            mod_pieces.at[owner],
            mod_pieces.at[owner],
            piece_send.at[k],
            piece_recv.at[owner],
            tp=lax.rem(t + k, tp_size),
        )

    for k in range(1, sp_size):
        part_copy(k, s).start()
    for k in range(1, sp_size):
        part_copy(k, lax.rem(s + k, sp_size)).wait_recv()
    total = mod_parts[0]
    for i in range(1, sp_size):
        total = total + mod_parts[i]
    mod_pieces[t] = total
    for k in range(1, tp_size):
        piece_copy(k, t).start()

    def forward(d):
        left = z - d
        right = z + d

        for part in range(2):

            @pl.when(left >= 0)
            def _():
                token_copy(2, left, c, part).wait_recv()

                @pl.when(z + 1 < chips)
                def _():
                    token_copy(0, left, c, part).start()

                token_copy(2, left, c, part).start()

            @pl.when(right < chips)
            def _():
                token_copy(2, right, c, part).wait_recv()

                @pl.when(z > 0)
                def _():
                    token_copy(1, right, c, part).start()

                token_copy(2, right, c, part).start()

    forward(1)
    for k in range(1, tp_size):
        piece_copy(k, lax.rem(t + k, tp_size)).wait_recv()
    for i in range(tp_size):
        mod_rows[:, i * piece : (i + 1) * piece] = mod_pieces[i]
    gate[...] = mod_rows[4:5, :]

    def normalise(source, base, count, row):
        def group(i, carry):
            x = source[aligned(base + i * ROWS, ROWS, ROWS), :].astype(jnp.float32)
            x = x - jnp.sum(x, axis=1, keepdims=True) * (1.0 / width)
            spread = jnp.sum(x * x, axis=1, keepdims=True) * (1.0 / width)
            y = x * lax.rsqrt(spread + EPSILON)
            y = y * (1.0 + mod_rows[2 + row : 3 + row, :]) + mod_rows[row : row + 1, :]
            normed[aligned(i * ROWS, ROWS, ROWS), :] = y.astype(jnp.bfloat16)
            return carry

        lax.fori_loop(0, count // ROWS, group, 0)

    my_head = lax.rem(s, heads)

    def mate(k):
        return lax.rem(my_head + k, heads)

    def kv_place(owner, b, is_context):
        if is_context:
            return aligned(owner * ctx_rows, ctx_rows, ROWS)
        return aligned(ctx_total + owner * block_tokens + b * pair, pair, ROWS)

    def stage_place(b, is_context):
        if is_context:
            return aligned(block_tokens, ctx_rows, ROWS)
        return aligned(b * pair, pair, ROWS)

    def kv_copy(k, owner, b, is_context):
        to = lax.rem(s + k, sp_size)
        return remote(
            kv_stage.at[lax.rem(to, heads), stage_place(b, is_context)],
            keys_values.at[kv_place(owner, b, is_context)],
            kv_send.at[k, b],
            kv_recv.at[owner, b],
            sp=to,
        )

    def q_copy(k, slot, b):
        place = aligned(b * pair, pair, ROWS)
        return remote(
            q_stage.at[mate(k), place],
            queries.at[slot, place],
            q_send.at[k, b],
            q_recv.at[slot, b],
            sp=s - my_head + mate(k),
        )

    def out_copy(k, head_index):
        return remote(
            out_stage.at[mate(k)],
            attended.at[head_index],
            out_send.at[k],
            out_recv.at[head_index],
            sp=s - my_head + mate(k),
        )

    def hand_out(keys, values, b, is_context):
        place = stage_place(b, is_context)
        for g in range(heads):
            kv_stage[g, place, :head] = keys[:, g * head : (g + 1) * head]
            kv_stage[g, place, head:] = values[:, g * head : (g + 1) * head]
        for k in range(1, sp_size):
            kv_copy(k, s, b, is_context).start()
        keys_values[kv_place(s, b, is_context), :] = kv_stage[my_head, place, :]

    locals_[1].wait()
    for i in (3, 4, 5):
        locals_[i].wait()

    quarter = half // 4
    lane = lax.broadcasted_iota(jnp.int32, (pair, half), 1)
    low = lax.rem(lane, 2 * quarter) < quarter

    def turn(raw, b):
        cos = cosine[aligned(b * pair, pair, ROWS), :]
        sin = sine[aligned(b * pair, pair, ROWS), :]
        parts = []
        for i in range(local // half):
            v = raw[:, i * half : (i + 1) * half].astype(jnp.bfloat16).astype(jnp.float32)
            other = jnp.where(low, pltpu.roll(v, half - quarter, 1), pltpu.roll(v, quarter, 1))
            parts.append((v * cos + other * sin).astype(jnp.bfloat16))
        return jnp.concatenate(parts, axis=1)

    def process(b):
        for part in range(2):
            token_copy(2, b, 1 - c, part).wait_recv()
        normalise(tokens, b * pair, pair, 0)
        x = normed[:pair, :]
        hand_out(
            turn(jnp.dot(x, wk[...], preferred_element_type=jnp.float32), b),
            jnp.dot(x, wv[...], preferred_element_type=jnp.float32).astype(jnp.bfloat16),
            b,
            False,
        )
        turned = turn(jnp.dot(x, wq[...], preferred_element_type=jnp.float32), b)
        place = aligned(b * pair, pair, ROWS)
        for g in range(heads):
            q_stage[g, place, :] = turned[:, g * head : (g + 1) * head]
        for k in range(1, heads):
            q_copy(k, my_head, b).start()
        queries[my_head, place, :] = q_stage[my_head, place, :]

    def process_context():
        locals_[2].wait()
        normalise(context_tokens, 0, ctx_rows, 1)
        hand_out(
            jnp.dot(normed[:ctx_rows, :], wk[...], preferred_element_type=jnp.float32).astype(
                jnp.bfloat16
            ),
            jnp.dot(normed[:ctx_rows, :], wv[...], preferred_element_type=jnp.float32).astype(
                jnp.bfloat16
            ),
            chips,
            True,
        )

    def step(j, carry):
        d = lax.div(j, 2)
        side = lax.rem(j, 2)

        @pl.when(j == 1)
        def _():
            if chips > 2:
                forward(2)
            process_context()

        @pl.when((side == 0) & (d >= 2) & (d + 1 < chips))
        def _():
            forward(d + 1)

        b = z - d + 2 * d * side

        @pl.when((b >= 0) & (b < chips) & (d + 1 > side))
        def _():
            process(b)

        return carry

    lax.fori_loop(0, 2 * chips, step, 0)

    for k in range(1, sp_size):
        owner = lax.rem(s + k, sp_size)
        kv_copy(k, owner, chips, True).wait_recv()
        for b in range(chips):
            kv_copy(k, owner, b, False).wait_recv()
    for k in range(1, heads):
        for b in range(chips):
            q_copy(k, mate(k), b).wait_recv()

    tile = min(256, block_tokens)
    key_total = keys_values.shape[0]
    factor = half ** (-0.5) * LOG2E
    on_context = lax.broadcasted_iota(jnp.int32, (1, key_total), 1) < ctx_total

    raised = jnp.where(on_context, lift[my_head] * LOG2E, 0.0)
    weight_of_second = lambdas[my_head]

    def attention(i, slot):
        place = aligned(i * tile, tile, ROWS)
        outs = []
        for m in range(2):
            scores = lax.dot_general(
                queries[slot, place, m * half : (m + 1) * half],
                keys_values[:, m * half : (m + 1) * half],
                (((1,), (1,)), ((), ())),
                preferred_element_type=jnp.float32,
            )
            scores = scores * factor + raised
            weights = jnp.exp2(scores - jnp.max(scores, axis=1, keepdims=True))
            sums = jnp.sum(weights, axis=1, keepdims=True)
            outs.append(
                jnp.dot(
                    weights.astype(jnp.bfloat16),
                    keys_values[:, head:],
                    preferred_element_type=jnp.float32,
                )
                / sums
            )
        diff = outs[0] - weight_of_second * outs[1]
        mean = jnp.sum(diff * diff, axis=1, keepdims=True) * (1.0 / head)
        out_stage[slot, place, :] = (diff * lax.rsqrt(mean + EPSILON) * gain[...]).astype(
            jnp.bfloat16
        )
        return slot

    for k in range(1, heads + 1):
        lax.fori_loop(0, block_tokens // tile, attention, mate(k))
        if k < heads:
            out_copy(k, my_head).start()
    attended[my_head] = out_stage[my_head]
    for k in range(1, heads):
        out_copy(k, mate(k)).wait_recv()
        out_copy(k, my_head).wait_send()
        for b in range(chips):
            q_copy(k, my_head, b).wait_send()

    for b in range(chips):
        for part in range(2):

            @pl.when((b <= z) & (z + 1 < chips))
            def _():
                token_copy(0, b, c, part).wait_send()

            @pl.when((b >= z) & (z > 0))
            def _():
                token_copy(1, b, c, part).wait_send()

            token_copy(2, b, c, part).wait_send()
    for k in range(1, tp_size):
        piece_copy(k, t).wait_send()
    for k in range(1, sp_size):
        part_copy(k, s).wait_send()
        kv_copy(k, s, chips, True).wait_send()
        for b in range(chips):
            kv_copy(k, s, b, False).wait_send()


def output_kernel(
    tp_size,
    attended,
    output_weight,
    latent,
    gate,
    result,
    weight,
    own,
    pair_send,
    pair_recv,
    stage,
    from_left,
    from_right,
    local_sem,
    ps_sem,
    pr_sem,
    st_sem,
    left_sem,
    right_sem,
):
    t = lax.axis_index("tp")
    z = lax.div(t, 2)
    c = lax.rem(t, 2)
    chips = tp_size // 2
    rows, width = latent.shape
    span = width // 2
    chunk = min(1024, span)

    load = pltpu.make_async_copy(output_weight, weight, local_sem)
    load.start()
    barrier = pltpu.get_barrier_semaphore()

    @pl.when(z > 0)
    def _():
        pl.semaphore_signal(barrier, inc=1, device_id={"tp": t - 2}, device_id_type=MESH)

    @pl.when(z + 1 < chips)
    def _():
        pl.semaphore_signal(barrier, inc=1, device_id={"tp": t + 2}, device_id_type=MESH)

    pl.semaphore_signal(barrier, inc=1, device_id={"tp": t + 1 - 2 * c}, device_id_type=MESH)
    inner = (z > 0) & (z + 1 < chips)
    pl.semaphore_wait(barrier, jnp.where(inner, 3, 2) if chips > 1 else 1)

    load.wait()

    def pair_copy(b):
        return remote(
            pair_send.at[b], pair_recv.at[b], ps_sem.at[b], pr_sem.at[b], tp=t + 1 - 2 * c
        )

    def right_copy(b):
        return remote(stage.at[b], from_left.at[b], st_sem.at[b], left_sem.at[b], tp=t + 2)

    def left_copy(b):
        return remote(stage.at[b], from_right.at[b], st_sem.at[b], right_sem.at[b], tp=t - 2)

    def compute(b, part):
        u = 2 * b + part
        other = aligned((2 * b + 1 - c) * rows, rows, ROWS)
        mine = aligned((2 * b + c) * rows, rows, ROWS)
        both = jnp.concatenate(
            [
                jnp.concatenate([attended[g, part, :] for g in range(attended.shape[0])], axis=1)
                for part in (other, mine)
            ],
            axis=0,
        )
        for n in range(span // chunk):
            cols = slice(n * chunk, (n + 1) * chunk)
            found = jnp.dot(
                both,
                weight[:, aligned(part * span + n * chunk, chunk, 128)],
                preferred_element_type=jnp.float32,
            )
            pair_send[u, :, cols] = found[:rows].astype(jnp.bfloat16)
            own[u, :, cols] = found[rows:]
        pair_copy(u).start()

    def combine(b, part):
        u = 2 * b + part
        pair_copy(u).wait_recv()

        @pl.when(b > z)
        def _():
            @pl.when(z > 0)
            def _():
                right_copy(u).wait_recv()
                stage[u] = (
                    own[u] + pair_recv[u].astype(jnp.float32) + from_left[u].astype(jnp.float32)
                ).astype(jnp.bfloat16)

            @pl.when(z == 0)
            def _():
                stage[u] = (own[u] + pair_recv[u].astype(jnp.float32)).astype(jnp.bfloat16)

            right_copy(u).start()

        @pl.when(b < z)
        def _():
            @pl.when(z + 1 < chips)
            def _():
                left_copy(u).wait_recv()
                stage[u] = (
                    own[u] + pair_recv[u].astype(jnp.float32) + from_right[u].astype(jnp.float32)
                ).astype(jnp.bfloat16)

            @pl.when(z + 1 == chips)
            def _():
                stage[u] = (own[u] + pair_recv[u].astype(jnp.float32)).astype(jnp.bfloat16)

            left_copy(u).start()

    def place_of(j):
        d = chips - 1 - lax.div(j, 4)
        side = lax.rem(lax.div(j, 2), 2)
        b = z - d + 2 * d * side
        return b, lax.rem(j, 2), (b >= 0) & (b < chips) & (d + 1 > side)

    at_end = (z == 0) | (z + 1 == chips)

    def first_pass(j, carry):
        b, part, valid = place_of(j)

        @pl.when(valid)
        def _():
            compute(b, part)

            @pl.when(at_end & (b != z))
            def _():
                combine(b, part)

        return carry

    lax.fori_loop(0, 4 * chips, first_pass, 0)

    def second_pass(j, carry):
        b, part, valid = place_of(j)

        @pl.when(valid & jnp.logical_not(at_end) & (b != z))
        def _():
            combine(b, part)

        return carry

    lax.fori_loop(0, 4 * chips, second_pass, 0)

    for part in range(2):
        u = 2 * z + part
        cols = slice(part * span, (part + 1) * span)
        pair_copy(u).wait_recv()
        own[u] = own[u] + pair_recv[u].astype(jnp.float32)

        @pl.when(z > 0)
        def _():
            right_copy(u).wait_recv()
            own[u] = own[u] + from_left[u].astype(jnp.float32)

        @pl.when(z + 1 < chips)
        def _():
            left_copy(u).wait_recv()
            own[u] = own[u] + from_right[u].astype(jnp.float32)

        result[:, cols] = (latent[:, cols].astype(jnp.float32) + gate[:, cols] * own[u]).astype(
            jnp.bfloat16
        )

    for u in range(2 * chips):
        pair_copy(u).wait_send()

        @pl.when(u // 2 > z)
        def _():
            right_copy(u).wait_send()

        @pl.when(u // 2 < z)
        def _():
            left_copy(u).wait_send()


def tables(places, half):
    quarter = half // 4
    inverse = ROPE_BASE ** (-jnp.arange(quarter, dtype=jnp.float32) / quarter)
    by_row = (places // GRID_W).astype(jnp.float32)[:, None] * inverse
    by_col = (places % GRID_W).astype(jnp.float32)[:, None] * inverse
    angles = jnp.concatenate([by_row, by_row, by_col, by_col], axis=1)
    sign = jnp.where(jnp.arange(half) % (2 * quarter) < quarter, -1.0, 1.0)
    return jnp.cos(angles), jnp.sin(angles) * sign


def shards(
    sp_size,
    tp_size,
    latent,
    context,
    condition,
    context_condition,
    modulation,
    query_weight,
    key_weight,
    value_weight,
    lambdas,
    context_lift,
    head_gain,
    output_weight,
):
    rows, width = latent.shape
    chips = tp_size // 2
    local = query_weight.shape[1]
    heads = lambdas.shape[0]
    head = local // heads
    half = head // 2
    block_tokens = rows * tp_size
    ctx_rows = context.shape[0]
    piece = modulation.shape[2]
    places = lax.axis_index("sp") * block_tokens + jnp.arange(block_tokens, dtype=jnp.int32)
    cosine, sine = tables(places, half)
    vmem = pl.BlockSpec(memory_space=pltpu.VMEM)
    smem = pl.BlockSpec(memory_space=pltpu.SMEM)
    anywhere = pl.BlockSpec(memory_space=pl.ANY)
    bf16, f32 = jnp.bfloat16, jnp.float32
    dma = pltpu.SemaphoreType.DMA
    attended, gate = pl.pallas_call(
        functools.partial(attend_kernel, sp_size, tp_size),
        out_shape=(
            jax.ShapeDtypeStruct((heads, block_tokens, head), bf16),
            jax.ShapeDtypeStruct((1, width), f32),
        ),
        in_specs=[anywhere] * 2 + [vmem] * 2 + [anywhere] * 4 + [vmem] * 2 + [smem] * 2 + [vmem],
        out_specs=(vmem, vmem),
        scratch_shapes=[
            pltpu.VMEM((block_tokens, width), bf16),
            pltpu.VMEM(context.shape, bf16),
            pltpu.VMEM((max(2 * rows, ctx_rows), width), bf16),
            pltpu.VMEM(modulation.shape, bf16),
            pltpu.VMEM((width, local), bf16),
            pltpu.VMEM((width, local), bf16),
            pltpu.VMEM((width, local), bf16),
            pltpu.VMEM((sp_size * (ctx_rows + block_tokens), 2 * head), bf16),
            pltpu.VMEM((heads, block_tokens, head), bf16),
            pltpu.VMEM((heads, block_tokens + ctx_rows, 2 * head), bf16),
            pltpu.VMEM((heads, block_tokens, head), bf16),
            pltpu.VMEM((heads, block_tokens, head), bf16),
            pltpu.VMEM((sp_size, 8, piece), f32),
            pltpu.VMEM((tp_size, 8, piece), f32),
            pltpu.VMEM((8, width), f32),
            dma((6,)),
            dma((3, 2 * chips)),
            dma((2 * tp_size,)),
            dma((sp_size,)),
            dma((sp_size,)),
            dma((tp_size,)),
            dma((tp_size,)),
            dma((sp_size, chips + 1)),
            dma((sp_size, chips + 1)),
            dma((heads, chips)),
            dma((heads, chips)),
            dma((heads,)),
            dma((heads,)),
        ],
        compiler_params=pltpu.CompilerParams(
            collective_id=0, has_side_effects=True, vmem_limit_bytes=VMEM_LIMIT
        ),
        name="attend",
    )(
        latent,
        context,
        condition.reshape(1, -1),
        context_condition.reshape(1, -1),
        modulation,
        query_weight,
        key_weight,
        value_weight,
        cosine,
        sine,
        lambdas,
        context_lift,
        head_gain.reshape(1, -1),
    )
    blocks = (2 * chips, rows, width // 2)
    return pl.pallas_call(
        functools.partial(output_kernel, tp_size),
        out_shape=jax.ShapeDtypeStruct((rows, width), bf16),
        in_specs=[vmem, anywhere, vmem, vmem],
        out_specs=vmem,
        scratch_shapes=[
            pltpu.VMEM(output_weight.shape, bf16),
            pltpu.VMEM(blocks, f32),
            pltpu.VMEM(blocks, bf16),
            pltpu.VMEM(blocks, bf16),
            pltpu.VMEM(blocks, bf16),
            pltpu.VMEM(blocks, bf16),
            pltpu.VMEM(blocks, bf16),
            dma(()),
            dma((2 * chips,)),
            dma((2 * chips,)),
            dma((2 * chips,)),
            dma((2 * chips,)),
            dma((2 * chips,)),
        ],
        compiler_params=pltpu.CompilerParams(
            collective_id=1, has_side_effects=True, vmem_limit_bytes=VMEM_LIMIT
        ),
        name="output",
    )(attended, output_weight, latent, gate)


def solution(mesh):
    in_specs = (
        P(("sp", "tp"), None),
        P("sp", None),
        P(),
        P(),
        P(None, "sp", "tp"),
        P(None, "tp"),
        P(None, "tp"),
        P(None, "tp"),
        P("tp"),
        P("tp"),
        P(),
        P("tp", None),
    )
    out_specs = P(("sp", "tp"), None)
    body = functools.partial(shards, mesh.shape["sp"], mesh.shape["tp"])
    return jax.shard_map(body, mesh=mesh, in_specs=in_specs, out_specs=out_specs, check_vma=False)
```

profile of v0, /device:TPU:0, one launch (start us, length us, event | category | flops | bytes accessed | tf_op | source)
XLA Modules:
  0.0 121.0 jit_solution(2677286851856377758)
XLA Ops:
  0.0 0.2 broadcast_multiply_fusion.1
  0.2 1.9 %sine_multiply_fusion = (f32[512,128]{1,0:T(8,128)}, f32[512,128]{1,0:T(8,128)}) fusion(f32[128]{0:T(128)S(1)} %compare_select_fusion, f32[512,32]{1,0:T(8,128)S(1)} %get-tuple-element.12, f32[512,32]{1,0:T(8,128)S(1)} %get-tuple-element.11), kind=kLoop, calls=%fused_computation.1 | loop fusion | flops 262144 | bytes 655872 | tf_op jit(solution)/shard_map/mul | solution.py:634
  2.1 78.0 %attend.1 = (bf16[2,512,256]{2,1,0:T(8,128)(2,1)}, f32[1,4096]{1,0:T(1,128)}) custom-call(bf16[64,4096]{1,0:T(8,128)(2,1)} %latent.3, bf16[128,4096]{1,0:T(8,128)(2,1)} %context.1, f32[1,4096]{1,0:T(1,128)} %bitcast.3, f32[1,4096]{1,0:T(1,128)} %bitcast.4, bf16[3,1024,512]{2,1,0:T(8,128)(2,1)} %modulation.1, bf16[4096,512]{1,0:T(8,128)(2,1)} %query_weight.1, ...), custom_call_target="tpu_custom_call" | custom-call | tf_op jit(solution)/shard_map/attend/pallas_call | solution.py:669
  80.1 39.0 %output.1 = bf16[64,4096]{1,0:T(8,128)(2,1)} custom-call(bf16[2,512,256]{2,1,0:T(8,128)(2,1)} %get-tuple-element.7.attended, bf16[512,4096]{1,0:T(8,128)(2,1)} %output_weight.1, bf16[64,4096]{1,0:T(8,128)(2,1)} %latent.3, f32[1,4096]{1,0:T(1,128)} %get-tuple-element.8.gate), custom_call_target="tpu_custom_call" | custom-call | tf_op jit(solution)/shard_map/output/pallas_call | solution.py:727
  119.1 1.9 %copy.14 = bf16[64,4096]{1,0:T(8,128)(2,1)} copy(bf16[64,4096]{1,0:T(8,128)(2,1)} %output.1) | data formatting | bytes 1048576
  (3 shorter events, 0.0 us)
where the time goes:
time: 122 us; the launch traced here: 121 us
  Pallas kernels  117 us (96%)
  other arithmetic  2.09 us (2%)
  local copies, waits for them, and re-layouts  1.87 us (2%)
    pallas_call x1, Pallas kernels, shards(): pl.pallas_call(functools.partial(attend_kernel, sp_size, tp_size), out_sh...  78 us
    pallas_call x1, Pallas kernels, shards(): pl.pallas_call(functools.partial(output_kernel, tp_size), out_shape=jax.S...  39 us

commit v1 on v0

v1 whole, which is shorter than its diff:
```python
import functools

import jax
import jax.numpy as jnp
import numpy as np
from jax import lax
from jax.experimental import pallas as pl
from jax.experimental.pallas import tpu as pltpu
from jax.sharding import PartitionSpec as P

GRID_W = 64
ROPE_BASE = 10000.0
EPSILON = 1e-05
LOG2E = 1.4426950408889634
ROWS = 16
LANES = 128
UNITS = 4
VMEM_LIMIT = 62 * 1024 * 1024
MESH = pl.DeviceIdType.MESH


def remote(src, dst, send_sem, recv_sem, **where):
    return pltpu.make_async_remote_copy(
        src_ref=src,
        dst_ref=dst,
        send_sem=send_sem,
        recv_sem=recv_sem,
        device_id=where,
        device_id_type=MESH,
    )


def aligned(start, size, unit):
    return pl.ds(pl.multiple_of(start, unit), size)


def block_kernel(
    sp_size,
    tp_size,
    latent,
    context,
    condition,
    context_condition,
    modulation,
    query_weight,
    key_weight,
    value_weight,
    tables,
    lambdas,
    lift,
    gain_in,
    output_weight,
    result,
    tokens,
    context_tokens,
    normed,
    mod_weight,
    wq,
    wk,
    wv,
    weight,
    keys_values,
    queries,
    kv_stage,
    q_stage,
    out_stage,
    attended,
    own,
    stage,
    from_left,
    from_right,
    mod_parts,
    mod_pieces,
    mod_rows,
    vectors_in,
    table,
    cosine,
    sine,
    gain,
    per_head,
    local_sem,
    tok_send,
    tok_recv,
    part_send,
    part_recv,
    piece_send,
    piece_recv,
    kv_send,
    kv_twin,
    kv_recv,
    q_send,
    q_recv,
    out_send,
    out_recv,
    wo_sem,
    head_sem,
    stage_sem,
    left_sem,
    right_sem,
):
    s = lax.axis_index("sp")
    t = lax.axis_index("tp")
    z = lax.div(t, 2)
    c = lax.rem(t, 2)
    twin = t + 1 - 2 * c
    chips = tp_size // 2
    rows, width = latent.shape
    parts = rows // ROWS
    half_rows = rows // 2
    half_parts = parts // 2
    pair = 2 * rows
    block_tokens = tp_size * rows
    ctx_rows = context.shape[0]
    ctx_total = ctx_rows * sp_size
    local = query_weight.shape[1]
    heads = lambdas.shape[0]
    head = local // heads
    half = head // 2
    plane = 2 * heads
    piece = modulation.shape[2]
    depth = modulation.shape[1]
    my_head = lax.rem(s, plane)
    base = s - my_head
    owner_core = lax.div(my_head, heads)
    mine = lax.rem(my_head, heads)
    is_owner = c == owner_core
    ctx_item = 2 * chips

    def load(i, src, dst):
        return pltpu.make_async_copy(src, dst, local_sem.at[i])

    own_slot = tokens.at[aligned(t * rows, rows, ROWS)]
    local_rows = aligned(c * local, local, ROWS)
    here = aligned(s * depth, depth, LANES)
    first_loads = [
        load(0, condition.at[:, here], vectors_in.at[0:1]),
        load(1, context_condition.at[:, here], vectors_in.at[1:2]),
        load(2, modulation, mod_weight),
    ]
    later_loads = [
        load(3, latent, own_slot),
        load(4, context, context_tokens),
        load(5, key_weight, wk),
        load(6, value_weight, wv),
        load(7, tables, table),
        load(8, query_weight, wq),
        load(9, gain_in, gain),
        load(10, output_weight, weight.at[local_rows]),
    ]
    barrier = pltpu.get_barrier_semaphore()
    for k in range(1, tp_size):
        pl.semaphore_signal(
            barrier, inc=1, device_id={"tp": lax.rem(t + k, tp_size)}, device_id_type=MESH
        )
    for k in range(1, sp_size):
        for to in (t, twin):
            pl.semaphore_signal(
                barrier,
                inc=1,
                device_id={"sp": lax.rem(s + k, sp_size), "tp": to},
                device_id_type=MESH,
            )
    for copy in first_loads + later_loads[:-1]:
        copy.start()
    for g in range(heads):
        per_head[c, 2 * g : 2 * g + 1, :] = jnp.full((1, LANES), lambdas[g], jnp.float32)
        per_head[c, 2 * g + 1 : 2 * g + 2, :] = jnp.full((1, LANES), lift[g], jnp.float32)
    pl.semaphore_wait(barrier, tp_size - 1 + 2 * (sp_size - 1))

    def token_copy(kind, b, core, part, mine_first=False):
        slot = 2 * b + core
        place = tokens.at[aligned(slot * rows + part * ROWS, ROWS, ROWS)]
        to = (t + 2, t - 2, twin)[kind]
        return remote(
            latent.at[aligned(part * ROWS, ROWS, ROWS)] if mine_first else place,
            place,
            tok_send.at[kind, parts * b + part],
            tok_recv.at[parts * slot + part],
            tp=to,
        )

    def send_mine(part):
        @pl.when(z + 1 < chips)
        def _():
            token_copy(0, z, c, part, True).start()

        @pl.when(z > 0)
        def _():
            token_copy(1, z, c, part, True).start()

        token_copy(2, z, c, part, True).start()

    for part in range(parts - 1):
        send_mine(part)

    first_loads[0].wait()
    first_loads[1].wait()
    v = vectors_in[...]
    v = v / (1.0 + jnp.exp(-v))
    which = lax.broadcasted_iota(jnp.int32, (ROWS, depth), 0)
    vectors = jnp.where(
        which == 0,
        jnp.broadcast_to(v[0:1], (ROWS, depth)),
        jnp.broadcast_to(v[1:2], (ROWS, depth)),
    ).astype(jnp.bfloat16)
    first_loads[2].wait()
    for r in range(3):
        found = jnp.dot(vectors, mod_weight[r], preferred_element_type=jnp.float32)
        mod_parts[s, 2 * r : 2 * r + 2, :] = found[0:2]
    mod_parts[s, 6:8, :] = jnp.zeros((2, piece), jnp.float32)

    def part_copy(k, owner):
        return remote(
            mod_parts.at[owner],
            mod_parts.at[owner],
            part_send.at[k],
            part_recv.at[owner],
            sp=lax.rem(s + k, sp_size),
        )

    def piece_copy(k, owner):
        return remote(
            mod_pieces.at[owner],
            mod_pieces.at[owner],
            piece_send.at[k],
            piece_recv.at[owner],
            tp=lax.rem(t + k, tp_size),
        )

    def head_copy(core):
        return remote(per_head.at[core], per_head.at[core], head_sem.at[0], head_sem.at[1], tp=twin)

    def weight_copy(core):
        return remote(
            output_weight,
            weight.at[aligned(core * local, local, ROWS)],
            wo_sem.at[0],
            wo_sem.at[1],
            tp=twin,
        )

    for k in range(1, sp_size):
        part_copy(k, s).start()
    head_copy(c).start()
    for k in range(1, sp_size):
        part_copy(k, lax.rem(s + k, sp_size)).wait_recv()
    total = mod_parts[0]
    for i in range(1, sp_size):
        total = total + mod_parts[i]
    mod_pieces[t] = total
    for k in range(1, tp_size):
        piece_copy(k, t).start()
    send_mine(parts - 1)
    later_loads[-1].start()
    weight_copy(c).start()

    def forward(d, part):
        left = z - d
        right = z + d

        @pl.when(left >= 0)
        def _():
            token_copy(2, left, c, part).wait_recv()

            @pl.when(z + 1 < chips)
            def _():
                token_copy(0, left, c, part).start()

            token_copy(2, left, c, part).start()

        @pl.when(right < chips)
        def _():
            token_copy(2, right, c, part).wait_recv()

            @pl.when(z > 0)
            def _():
                token_copy(1, right, c, part).start()

            token_copy(2, right, c, part).start()

    for part in range(parts - 1):
        forward(1, part)

    grid_rows = block_tokens // GRID_W
    all_rows = table.shape[1] - GRID_W
    later_loads[4].wait()
    is_row = lax.broadcasted_iota(jnp.int32, (GRID_W, half), 1) < half // 2
    for kind, into in enumerate((cosine, sine)):
        by_col = table[kind, all_rows:, :]
        for r in range(grid_rows):
            by_row = table[kind, pl.ds(s * grid_rows + r, 1), :]
            into[r * GRID_W : (r + 1) * GRID_W, :] = jnp.where(is_row, by_row, by_col)

    for k in range(1, tp_size):
        piece_copy(k, lax.rem(t + k, tp_size)).wait_recv()
    for i in range(tp_size):
        found = mod_pieces[i]
        mod_rows[0:2, i * piece : (i + 1) * piece] = found[0:2]
        mod_rows[2:4, i * piece : (i + 1) * piece] = 1.0 + found[2:4]
        mod_rows[4:6, i * piece : (i + 1) * piece] = found[4:6]

    tiles = width // LANES

    def normalise(pieces, row):
        def tile(ref, start, count, i):
            x = ref[aligned(start, count, ROWS), i * LANES : (i + 1) * LANES]
            return x.astype(jnp.float32)

        to = 0
        for ref, start, count in pieces:
            sums = tile(ref, start, count, 0)
            for i in range(1, tiles):
                sums = sums + tile(ref, start, count, i)
            center = jnp.sum(sums, axis=1, keepdims=True) * (1.0 / width)
            squares = jnp.zeros((count, LANES), jnp.float32)
            for i in range(tiles):
                x = tile(ref, start, count, i) - center
                squares = squares + x * x
            spread = jnp.sum(squares, axis=1, keepdims=True) * (1.0 / width)
            inverse = lax.rsqrt(spread + EPSILON)
            for i in range(tiles):
                cols = slice(i * LANES, (i + 1) * LANES)
                x = (tile(ref, start, count, i) - center) * inverse
                y = x * mod_rows[2 + row : 3 + row, cols] + mod_rows[row : row + 1, cols]
                normed[to : to + count, cols] = y.astype(jnp.bfloat16)
            to += count

    def kv_place(owner, item):
        return aligned(ctx_total + owner * block_tokens + item * rows, rows, ROWS)

    def ctx_place(owner):
        return aligned(owner * ctx_rows, ctx_rows, ROWS)

    def stage_place(item):
        return aligned(item * rows, rows, ROWS)

    ctx_stage = pl.ds(block_tokens, ctx_rows)

    def kv_copy(k, owner, item, is_context):
        to = lax.rem(s + k, sp_size)
        return remote(
            kv_stage.at[lax.rem(to, heads), ctx_stage if is_context else stage_place(item)],
            keys_values.at[ctx_place(owner) if is_context else kv_place(owner, item)],
            kv_send.at[k, item],
            kv_recv.at[owner, item],
            sp=to,
        )

    def wanted(k):
        to = lax.rem(s + k, sp_size)
        return lax.div(lax.rem(to, plane), heads) == c

    def twin_copy(owner, item, is_context):
        place = keys_values.at[ctx_place(owner) if is_context else kv_place(owner, item)]
        return remote(place, place, kv_twin.at[owner, item], kv_recv.at[owner, item], tp=twin)

    def hand_out(keys, values, item, is_context):
        place = ctx_stage if is_context else stage_place(item)
        for g in range(heads):
            kv_stage[g, place, :head] = keys[:, g * head : (g + 1) * head]
            kv_stage[g, place, head:] = values[:, g * head : (g + 1) * head]
        for k in range(1, sp_size):

            @pl.when(wanted(k))
            def _():
                kv_copy(k, s, item, is_context).start()

        @pl.when(is_owner)
        def _():
            to = ctx_place(s) if is_context else kv_place(s, item)
            keys_values[to, :] = kv_stage[mine, place, :]
            twin_copy(s, item, is_context).start()

    def pass_on(item, is_context):
        @pl.when(is_owner)
        def _():
            for k in range(1, sp_size):
                owner = lax.rem(s + k, sp_size)
                kv_copy(k, owner, item, is_context).wait_recv()
                twin_copy(owner, item, is_context).start()

    def q_copy(g, rel, source, item):
        core = c + rel - 2 * c * rel
        b = lax.div(item, 2)
        side = lax.rem(item, 2)
        return remote(
            q_stage.at[g, aligned(item * rows + core * half_rows, half_rows, ROWS)],
            queries.at[b, aligned(source * rows + side * half_rows, half_rows, ROWS)],
            q_send.at[2 * g + rel, item],
            q_recv.at[source, item],
            sp=base + c * heads + g,
            tp=twin if rel else t,
        )

    def out_copy(b, k, index):
        to = lax.rem(my_head + k, plane)
        return remote(
            out_stage.at[b, aligned(to * rows, rows, ROWS)],
            attended.at[b, index],
            out_send.at[b, k],
            out_recv.at[b, index],
            sp=base + to,
        )

    quarter = half // 4
    lane = lax.broadcasted_iota(jnp.int32, (rows, half), 1)
    low = lax.rem(lane, 2 * quarter) < quarter

    def turn(raw, b, side):
        def of(ref):
            return jnp.concatenate(
                [
                    ref[aligned(b * pair + core * rows + side * half_rows, half_rows, ROWS), :]
                    for core in range(2)
                ],
                axis=0,
            )

        cos = of(cosine)
        sin = of(sine)
        found = []
        for i in range(local // half):
            v = raw[:, i * half : (i + 1) * half].astype(jnp.bfloat16).astype(jnp.float32)
            other = jnp.where(low, pltpu.roll(v, half - quarter, 1), pltpu.roll(v, quarter, 1))
            found.append((v * cos + other * sin).astype(jnp.bfloat16))
        return jnp.concatenate(found, axis=1)

    def process(b, side):
        item = 2 * b + side
        for i in range(half_parts):
            token_copy(2, b, 1 - c, side * half_parts + i).wait_recv()
        normalise(
            [(tokens, (2 * b + core) * rows + side * half_rows, half_rows) for core in range(2)], 0
        )
        x = normed[:rows, :]
        hand_out(
            turn(jnp.dot(x, wk[...], preferred_element_type=jnp.float32), b, side),
            jnp.dot(x, wv[...], preferred_element_type=jnp.float32).astype(jnp.bfloat16),
            item,
            False,
        )
        turned = turn(jnp.dot(x, wq[...], preferred_element_type=jnp.float32), b, side)
        for g in range(heads):
            q_stage[g, stage_place(item), :] = turned[:, g * head : (g + 1) * head]
            for rel in range(2):
                if rel:
                    q_copy(g, rel, my_head, item).start()
                else:

                    @pl.when(c * heads + g != my_head)
                    def _():
                        q_copy(g, rel, my_head, item).start()

                    @pl.when(c * heads + g == my_head)
                    def _():
                        queries[
                            b, aligned(my_head * rows + side * half_rows, half_rows, ROWS), :
                        ] = q_stage[g, aligned(item * rows + c * half_rows, half_rows, ROWS), :]

    for i in (1, 2, 3):
        later_loads[i].wait()
    step_rows = min(ctx_rows, 2 * ROWS)

    def context_group(i, carry):
        normalise_context(i)
        return carry

    def normalise_context(i):
        start = i * step_rows
        x = context_tokens[aligned(start, step_rows, ROWS), :].astype(jnp.float32)
        x = x - jnp.sum(x, axis=1, keepdims=True) * (1.0 / width)
        spread = jnp.sum(x * x, axis=1, keepdims=True) * (1.0 / width)
        y = x * lax.rsqrt(spread + EPSILON) * mod_rows[3:4, :] + mod_rows[1:2, :]
        normed[aligned(start, step_rows, ROWS), :] = y.astype(jnp.bfloat16)

    lax.fori_loop(0, ctx_rows // step_rows, context_group, 0)
    hand_out(
        jnp.dot(normed[:ctx_rows, :], wk[...], preferred_element_type=jnp.float32).astype(
            jnp.bfloat16
        ),
        jnp.dot(normed[:ctx_rows, :], wv[...], preferred_element_type=jnp.float32).astype(
            jnp.bfloat16
        ),
        ctx_item,
        True,
    )
    forward(1, parts - 1)
    later_loads[0].wait()
    later_loads[5].wait()

    flip = jnp.where(2 * z >= chips, 0, 1)

    def step(j, last):
        d = lax.div(j, 4)
        turn_of = lax.rem(lax.div(j, 2), 2)
        side = lax.rem(j, 2)
        pick = turn_of + flip - 2 * turn_of * flip
        b = z - d + 2 * d * pick
        valid = (b >= 0) & (b < chips) & (d + 1 > turn_of)

        @pl.when(((d == 1) & (side == 0)) | ((d >= 3) & (turn_of == 0)))
        def _():
            which_half = jnp.where(d == 1, turn_of, side)
            for i in range(half_parts):
                forward(jnp.where(d == 1, 2, d), which_half * half_parts + i)

        @pl.when(valid)
        def _():
            process(b, side)

            @pl.when(j > 0)
            def _():
                pass_on(last, False)

        @pl.when(j == 0)
        def _():
            pass_on(ctx_item, True)

        return jnp.where(valid, 2 * b + side, last)

    last = lax.fori_loop(0, 4 * chips, step, 2 * z)
    pass_on(last, False)

    @pl.when(jnp.logical_not(is_owner))
    def _():
        def take(i, carry):
            twin_copy(lax.div(i, 2 * chips), lax.rem(i, 2 * chips), False).wait_recv()
            return carry

        lax.fori_loop(0, sp_size * 2 * chips, take, 0)

        def take_context(i, carry):
            twin_copy(i, ctx_item, True).wait_recv()
            return carry

        lax.fori_loop(0, sp_size, take_context, 0)

    head_copy(1 - c).wait_recv()
    weight_copy(1 - c).wait_recv()
    later_loads[6].wait()
    later_loads[7].wait()

    tile = plane * rows
    factor = half ** (-0.5) * LOG2E
    weight_of_second = per_head[owner_core, pl.ds(2 * mine, 1), :][:, 0:1]
    raised = per_head[owner_core, pl.ds(2 * mine + 1, 1), :][:, 0:1] * LOG2E

    def attention(b):
        for k in range(plane):
            source = lax.rem(my_head + k, plane)

            @pl.when(jnp.logical_or(k > 0, jnp.logical_not(is_owner)))
            def _():
                for side in range(2):
                    q_copy(0, 0, source, 2 * b + side).wait_recv()

        outs = []
        for m in range(2):
            scores = lax.dot_general(
                queries[b, :, m * half : (m + 1) * half],
                keys_values[:, m * half : (m + 1) * half],
                (((1,), (1,)), ((), ())),
                preferred_element_type=jnp.float32,
            )
            scores = jnp.concatenate(
                [scores[:, :ctx_total] * factor + raised, scores[:, ctx_total:] * factor], axis=1
            )
            weights = jnp.exp2(scores - jnp.max(scores, axis=1, keepdims=True))
            sums = jnp.sum(weights, axis=1, keepdims=True)
            outs.append(
                jnp.dot(
                    weights.astype(jnp.bfloat16),
                    keys_values[:, head:],
                    preferred_element_type=jnp.float32,
                )
                / sums
            )
        diff = outs[0] - weight_of_second * outs[1]
        mean = jnp.sum(diff * diff, axis=1, keepdims=True) * (1.0 / head)
        out_stage[b, :, :] = (diff * lax.rsqrt(mean + EPSILON) * gain[...]).astype(jnp.bfloat16)
        for k in range(1, plane):
            out_copy(b, k, my_head).start()
        attended[b, my_head] = out_stage[b, aligned(my_head * rows, rows, ROWS), :]

    span = width // UNITS
    at_end = (z == 0) | (z + 1 == chips)

    def right_copy(u):
        return remote(stage.at[u], from_left.at[u], stage_sem.at[u], left_sem.at[u], tp=t + 2)

    def left_copy(u):
        return remote(stage.at[u], from_right.at[u], stage_sem.at[u], right_sem.at[u], tp=t - 2)

    def project(b):
        for k in range(1, plane):
            out_copy(b, k, lax.rem(my_head + k, plane)).wait_recv()
        x = jnp.concatenate([attended[b, g] for g in range(plane)], axis=1)
        for n in range(UNITS):
            u = b * UNITS + n
            found = jnp.dot(
                x, weight[:, n * span : (n + 1) * span], preferred_element_type=jnp.float32
            )
            own[u] = found

            @pl.when(at_end & (b != z))
            def _():
                stage[u] = found.astype(jnp.bfloat16)

                @pl.when(z == 0)
                def _():
                    right_copy(u).start()

                @pl.when(z > 0)
                def _():
                    left_copy(u).start()

    near = jnp.minimum(z, chips - 1 - z)
    far = jnp.maximum(z, chips - 1 - z)

    def block_of(i):
        r = i - (far - near)
        single = r < 0
        dist = jnp.where(single, far - i, near - lax.div(jnp.maximum(r, 0), 2))
        turn_of = jnp.where(single, 0, lax.rem(jnp.maximum(r, 0), 2))
        pick = turn_of + flip - 2 * turn_of * flip
        return z - dist + 2 * dist * pick

    def attend_step(i, carry):
        @pl.when(i < chips)
        def _():
            attention(block_of(i))

        @pl.when(i > 0)
        def _():
            project(block_of(i - 1))

        return carry

    lax.fori_loop(0, chips + 1, attend_step, 0)

    hop = 2

    def combine_step(i, carry):
        q = i - hop * (chips - 1 - z)
        b = lax.div(jnp.maximum(q, 0), UNITS)

        @pl.when((q >= 0) & (b < z))
        def _():
            left_copy(q).wait_recv()
            stage[q] = (own[q] + from_right[q].astype(jnp.float32)).astype(jnp.bfloat16)
            left_copy(q).start()

        p = i - hop * z
        e = chips - 1 - lax.div(jnp.maximum(p, 0), UNITS)
        u = e * UNITS + lax.rem(jnp.maximum(p, 0), UNITS)

        @pl.when((p >= 0) & (e > z))
        def _():
            right_copy(u).wait_recv()
            stage[u] = (own[u] + from_left[u].astype(jnp.float32)).astype(jnp.bfloat16)
            right_copy(u).start()

        return carry

    @pl.when(jnp.logical_not(at_end))
    def _():
        lax.fori_loop(0, (chips - 1) * UNITS + hop * (chips - 1), combine_step, 0)

    for n in range(UNITS):
        u = z * UNITS + n
        cols = slice(n * span, (n + 1) * span)

        @pl.when(z > 0)
        def _():
            right_copy(u).wait_recv()
            own[u] = own[u] + from_left[u].astype(jnp.float32)

        @pl.when(z + 1 < chips)
        def _():
            left_copy(u).wait_recv()
            own[u] = own[u] + from_right[u].astype(jnp.float32)

        result[:, cols] = (
            tokens[aligned(t * rows, rows, ROWS), cols].astype(jnp.float32)
            + mod_rows[4:5, cols] * own[u]
        ).astype(jnp.bfloat16)

    def sent_stage(u, carry):
        @pl.when(lax.div(u, UNITS) != z)
        def _():
            left_copy(u).wait_send()

        return carry

    lax.fori_loop(0, UNITS * chips, sent_stage, 0)

    def sent_block(b, carry):
        for k in range(1, plane):
            out_copy(b, k, my_head).wait_send()
        for part in range(parts):

            @pl.when((b <= z) & (z + 1 < chips))
            def _():
                token_copy(0, b, c, part).wait_send()

            @pl.when((b >= z) & (z > 0))
            def _():
                token_copy(1, b, c, part).wait_send()

            token_copy(2, b, c, part).wait_send()
        return carry

    lax.fori_loop(0, chips, sent_block, 0)

    def sent_item(item, carry):
        for g in range(heads):
            q_copy(g, 1, my_head, item).wait_send()

            @pl.when(c * heads + g != my_head)
            def _():
                q_copy(g, 0, my_head, item).wait_send()

        for k in range(1, sp_size):

            @pl.when(wanted(k))
            def _():
                kv_copy(k, s, item, False).wait_send()

        @pl.when(is_owner)
        def _():
            for k in range(sp_size):
                twin_copy(k, item, False).wait_send()

        return carry

    lax.fori_loop(0, 2 * chips, sent_item, 0)
    for k in range(1, sp_size):
        part_copy(k, s).wait_send()

        @pl.when(wanted(k))
        def _():
            kv_copy(k, s, ctx_item, True).wait_send()

    @pl.when(is_owner)
    def _():
        for k in range(sp_size):
            twin_copy(k, ctx_item, True).wait_send()

    for k in range(1, tp_size):
        piece_copy(k, t).wait_send()
    head_copy(c).wait_send()
    weight_copy(c).wait_send()


def tables(grid_rows, half):
    quarter = half // 4
    inverse = (ROPE_BASE ** (-np.arange(quarter) / quarter)).astype(np.float32)
    sign = np.where(np.arange(half) % (2 * quarter) < quarter, -1.0, 1.0)
    places = np.concatenate([np.arange(grid_rows), np.arange(GRID_W)]).astype(np.float32)
    angles = (places[:, None] * np.tile(inverse, 4)).astype(np.float64)
    return np.stack([np.cos(angles), np.sin(angles) * sign]).astype(np.float32)


def shards(
    sp_size,
    tp_size,
    latent,
    context,
    condition,
    context_condition,
    modulation,
    query_weight,
    key_weight,
    value_weight,
    lambdas,
    context_lift,
    head_gain,
    output_weight,
):
    rows, width = latent.shape
    chips = tp_size // 2
    local = query_weight.shape[1]
    heads = lambdas.shape[0]
    head = local // heads
    half = head // 2
    plane = 2 * heads
    block_tokens = rows * tp_size
    ctx_rows = context.shape[0]
    piece = modulation.shape[2]
    depth = modulation.shape[1]
    parts = rows // ROWS
    table = tables(sp_size * block_tokens // GRID_W, half)
    vmem = pl.BlockSpec(memory_space=pltpu.VMEM)
    smem = pl.BlockSpec(memory_space=pltpu.SMEM)
    anywhere = pl.BlockSpec(memory_space=pl.ANY)
    bf16, f32 = jnp.bfloat16, jnp.float32
    dma = pltpu.SemaphoreType.DMA
    units = (UNITS * chips, rows, width // UNITS)
    return pl.pallas_call(
        functools.partial(block_kernel, sp_size, tp_size),
        out_shape=jax.ShapeDtypeStruct((rows, width), bf16),
        in_specs=[anywhere] * 9 + [smem] * 2 + [anywhere] * 2,
        out_specs=vmem,
        scratch_shapes=[
            pltpu.VMEM((block_tokens, width), bf16),
            pltpu.VMEM(context.shape, bf16),
            pltpu.VMEM((max(rows, ctx_rows), width), bf16),
            pltpu.VMEM(modulation.shape, bf16),
            pltpu.VMEM((width, local), bf16),
            pltpu.VMEM((width, local), bf16),
            pltpu.VMEM((width, local), bf16),
            pltpu.VMEM((2 * local, width), bf16),
            pltpu.VMEM((sp_size * (ctx_rows + block_tokens), 2 * head), bf16),
            pltpu.VMEM((chips, plane * rows, head), bf16),
            pltpu.VMEM((heads, block_tokens + ctx_rows, 2 * head), bf16),
            pltpu.VMEM((heads, block_tokens, head), bf16),
            pltpu.VMEM((chips, plane * rows, head), bf16),
            pltpu.VMEM((chips, plane, rows, head), bf16),
            pltpu.VMEM(units, f32),
            pltpu.VMEM(units, bf16),
            pltpu.VMEM(units, bf16),
            pltpu.VMEM(units, bf16),
            pltpu.VMEM((sp_size, 8, piece), f32),
            pltpu.VMEM((tp_size, 8, piece), f32),
            pltpu.VMEM((8, width), f32),
            pltpu.VMEM((2, depth), f32),
            pltpu.VMEM(table.shape, f32),
            pltpu.VMEM((block_tokens, half), f32),
            pltpu.VMEM((block_tokens, half), f32),
            pltpu.VMEM((1, head), f32),
            pltpu.VMEM((2, 8, LANES), f32),
            dma((11,)),
            dma((3, parts * chips)),
            dma((parts * tp_size,)),
            dma((sp_size,)),
            dma((sp_size,)),
            dma((tp_size,)),
            dma((tp_size,)),
            dma((sp_size, 2 * chips + 1)),
            dma((sp_size, 2 * chips + 1)),
            dma((sp_size, 2 * chips + 1)),
            dma((2 * heads, 2 * chips)),
            dma((plane, 2 * chips)),
            dma((chips, plane)),
            dma((chips, plane)),
            dma((2,)),
            dma((2,)),
            dma((UNITS * chips,)),
            dma((UNITS * chips,)),
            dma((UNITS * chips,)),
        ],
        compiler_params=pltpu.CompilerParams(
            collective_id=0, has_side_effects=True, vmem_limit_bytes=VMEM_LIMIT
        ),
        name="block",
    )(
        latent,
        context,
        condition.reshape(1, -1),
        context_condition.reshape(1, -1),
        modulation,
        query_weight,
        key_weight,
        value_weight,
        table,
        lambdas,
        context_lift,
        head_gain.reshape(1, -1),
        output_weight,
    )


def solution(mesh):
    in_specs = (
        P(("sp", "tp"), None),
        P("sp", None),
        P(),
        P(),
        P(None, "sp", "tp"),
        P(None, "tp"),
        P(None, "tp"),
        P(None, "tp"),
        P("tp"),
        P("tp"),
        P(),
        P("tp", None),
    )
    out_specs = P(("sp", "tp"), None)
    body = functools.partial(shards, mesh.shape["sp"], mesh.shape["tp"])
    return jax.shard_map(body, mesh=mesh, in_specs=in_specs, out_specs=out_specs, check_vma=False)
```

time: 122 us -> 103 us (0.84)
  Pallas kernels: 117 us -> 100 us
  other arithmetic: 2.09 us -> 0 us
    pallas_call x2 -> x1, Pallas kernels: 117 us -> 100 us  [shards(): pl.pallas_call(functools.partial(block_kernel, sp_size, tp_size), out_sha...]
    mul x2 -> x0, other arithmetic: 2.06 us -> none  [the longest x1 1.86 us: tables(): return (jnp.cos(angles), jnp.sin(angles) * sign)]
where the time goes in v1:
time: 103 us; the launch traced here: 102 us
  Pallas kernels  100 us (97%)
  local copies, waits for them, and re-layouts  1.87 us (2%)
    pallas_call x1, Pallas kernels, shards(): pl.pallas_call(functools.partial(block_kernel, sp_size, tp_size), out_sha...  100 us

profile of v1, /device:TPU:0, one launch (start us, length us, event | category | flops | bytes accessed | tf_op | source)
XLA Modules:
  0.0 102.0 jit_solution(13363510274941357888)
XLA Ops:
  0.0 100.1 %block.1 = bf16[64,4096]{1,0:T(8,128)(2,1)} custom-call(bf16[64,4096]{1,0:T(8,128)(2,1)} %latent.1, bf16[128,4096]{1,0:T(8,128)(2,1)} %context.1, f32[1,4096]{1,0:T(1,128)} %bitcast.3, f32[1,4096]{1,0:T(1,128)} %bitcast.4, bf16[3,1024,512]{2,1,0:T(8,128)(2,1)} %modulation.1, bf16[4096,512]{1,0:T(8,128)(2,1)} %query_weight.1, bf16[4096,512]{1,0:T(8,128)(2,1)} %key_weight.1, ...), custom_call_target="tpu_custom_call" | custom-call | tf_op jit(solution)/shard_map/block/pallas_call | solution.py:799
  100.1 1.9 %copy.15 = bf16[64,4096]{1,0:T(8,128)(2,1)} copy(bf16[64,4096]{1,0:T(8,128)(2,1)} %block.1) | data formatting | bytes 1048576

commit v2 on v1

v2 whole, which is shorter than its diff:
```python
import functools

import jax
import jax.numpy as jnp
import numpy as np
from jax import lax
from jax.experimental import pallas as pl
from jax.experimental.pallas import tpu as pltpu
from jax.sharding import PartitionSpec as P

GRID_W = 64
ROPE_BASE = 10000.0
EPSILON = 1e-05
LOG2E = 1.4426950408889634
ROWS = 16
LANES = 128
UNITS = 4
VMEM_LIMIT = 62 * 1024 * 1024
MESH = pl.DeviceIdType.MESH


def remote(src, dst, send_sem, recv_sem, **where):
    return pltpu.make_async_remote_copy(
        src_ref=src,
        dst_ref=dst,
        send_sem=send_sem,
        recv_sem=recv_sem,
        device_id=where,
        device_id_type=MESH,
    )


def aligned(start, size, unit):
    return pl.ds(pl.multiple_of(start, unit), size)


def block_kernel(
    sp_size,
    tp_size,
    latent,
    context,
    condition,
    context_condition,
    modulation,
    query_weight,
    key_weight,
    value_weight,
    tables,
    lambdas,
    lift,
    gain_in,
    output_weight,
    result,
    tokens,
    context_tokens,
    normed,
    mod_weight,
    wq,
    wk,
    wv,
    weight,
    keys_values,
    queries,
    kv_stage,
    q_stage,
    out_stage,
    attended,
    own,
    stage,
    from_left,
    from_right,
    mod_parts,
    mod_pieces,
    mod_rows,
    vectors_in,
    table,
    cosine,
    sine,
    gain,
    per_head,
    held,
    held_peak,
    held_sums,
    local_sem,
    tok_send,
    tok_recv,
    part_send,
    part_recv,
    piece_send,
    piece_recv,
    kv_send,
    kv_twin,
    kv_recv,
    kv_pass,
    q_send,
    q_recv,
    out_send,
    out_recv,
    wo_sem,
    head_sem,
    stage_sem,
    left_sem,
    right_sem,
):
    s = lax.axis_index("sp")
    t = lax.axis_index("tp")
    z = lax.div(t, 2)
    c = lax.rem(t, 2)
    twin = t + 1 - 2 * c
    chips = tp_size // 2
    rows, width = latent.shape
    parts = rows // ROWS
    half_rows = rows // 2
    half_parts = parts // 2
    pair = 2 * rows
    block_tokens = tp_size * rows
    ctx_rows = context.shape[0]
    ctx_total = ctx_rows * sp_size
    local = query_weight.shape[1]
    heads = lambdas.shape[0]
    head = local // heads
    half = head // 2
    plane = 2 * heads
    piece = modulation.shape[2]
    depth = modulation.shape[1]
    my_head = lax.rem(s, plane)
    base = s - my_head
    owner_core = lax.div(my_head, heads)
    mine = lax.rem(my_head, heads)
    is_owner = c == owner_core
    ctx_item = 2 * chips

    def load(i, src, dst):
        return pltpu.make_async_copy(src, dst, local_sem.at[i])

    own_slot = tokens.at[aligned(t * rows, rows, ROWS)]
    local_rows = aligned(c * local, local, ROWS)
    here = aligned(s * depth, depth, LANES)
    first_loads = [
        load(0, condition.at[:, here], vectors_in.at[0:1]),
        load(1, context_condition.at[:, here], vectors_in.at[1:2]),
        load(2, modulation, mod_weight),
    ]
    later_loads = [
        load(3, latent, own_slot),
        load(4, context, context_tokens),
        load(5, key_weight, wk),
        load(6, value_weight, wv),
        load(7, tables, table),
        load(8, query_weight, wq),
        load(9, gain_in, gain),
        load(10, output_weight, weight.at[local_rows]),
    ]
    barrier = pltpu.get_barrier_semaphore()
    for k in range(1, tp_size):
        pl.semaphore_signal(
            barrier, inc=1, device_id={"tp": lax.rem(t + k, tp_size)}, device_id_type=MESH
        )
    for k in range(1, sp_size):
        for to in (t, twin):
            pl.semaphore_signal(
                barrier,
                inc=1,
                device_id={"sp": lax.rem(s + k, sp_size), "tp": to},
                device_id_type=MESH,
            )
    for copy in first_loads + later_loads[:-1]:
        copy.start()
    for g in range(heads):
        per_head[c, 2 * g : 2 * g + 1, :] = jnp.full((1, LANES), lambdas[g], jnp.float32)
        per_head[c, 2 * g + 1 : 2 * g + 2, :] = jnp.full((1, LANES), lift[g], jnp.float32)
    pl.semaphore_wait(barrier, tp_size - 1 + 2 * (sp_size - 1))

    def token_copy(kind, b, core, part, mine_first=False):
        slot = 2 * b + core
        place = tokens.at[aligned(slot * rows + part * ROWS, ROWS, ROWS)]
        to = (t + 2, t - 2, twin)[kind]
        return remote(
            latent.at[aligned(part * ROWS, ROWS, ROWS)] if mine_first else place,
            place,
            tok_send.at[kind, 0 if kind == 2 else b],
            tok_recv.at[parts * slot + part],
            tp=to,
        )

    def send_mine(part):
        @pl.when(z + 1 < chips)
        def _():
            token_copy(0, z, c, part, True).start()

        @pl.when(z > 0)
        def _():
            token_copy(1, z, c, part, True).start()

        token_copy(2, z, c, part, True).start()

    for part in range(half_parts):
        send_mine(part)

    first_loads[0].wait()
    first_loads[1].wait()
    v = vectors_in[...]
    v = v / (1.0 + jnp.exp(-v))
    which = lax.broadcasted_iota(jnp.int32, (ROWS, depth), 0)
    vectors = jnp.where(
        which == 0,
        jnp.broadcast_to(v[0:1], (ROWS, depth)),
        jnp.broadcast_to(v[1:2], (ROWS, depth)),
    ).astype(jnp.bfloat16)
    first_loads[2].wait()
    for r in range(3):
        found = jnp.dot(vectors, mod_weight[r], preferred_element_type=jnp.float32)
        mod_parts[s, 2 * r : 2 * r + 2, :] = found[0:2]
    mod_parts[s, 6:8, :] = jnp.zeros((2, piece), jnp.float32)

    def part_copy(k, owner):
        return remote(
            mod_parts.at[owner],
            mod_parts.at[owner],
            part_send,
            part_recv.at[owner],
            sp=lax.rem(s + k, sp_size),
        )

    def piece_copy(k, owner):
        return remote(
            mod_pieces.at[owner],
            mod_pieces.at[owner],
            piece_send,
            piece_recv.at[owner],
            tp=lax.rem(t + 2 * k, tp_size),
        )

    def piece_across(owner):
        return remote(
            mod_pieces.at[owner],
            mod_pieces.at[owner],
            piece_send,
            piece_recv.at[owner],
            tp=twin,
        )

    def head_copy(core):
        return remote(per_head.at[core], per_head.at[core], head_sem.at[0], head_sem.at[1], tp=twin)

    def weight_copy(core):
        return remote(
            output_weight,
            weight.at[aligned(core * local, local, ROWS)],
            wo_sem.at[0],
            wo_sem.at[1],
            tp=twin,
        )

    for k in range(1, sp_size):
        part_copy(k, s).start()
    head_copy(c).start()
    for k in range(1, sp_size):
        part_copy(k, lax.rem(s + k, sp_size)).wait_recv()
    total = mod_parts[0]
    for i in range(1, sp_size):
        total = total + mod_parts[i]
    mod_pieces[t] = total
    for k in range(1, chips):
        piece_copy(k, t).start()
    piece_across(t).start()
    for part in range(half_parts, parts):
        send_mine(part)
    later_loads[-1].start()
    weight_copy(c).start()

    def forward(d, part):
        left = z - d
        right = z + d

        @pl.when(left >= 0)
        def _():
            token_copy(2, left, c, part).wait_recv()

            @pl.when(z + 1 < chips)
            def _():
                token_copy(0, left, c, part).start()

            token_copy(2, left, c, part).start()

        @pl.when(right < chips)
        def _():
            token_copy(2, right, c, part).wait_recv()

            @pl.when(z > 0)
            def _():
                token_copy(1, right, c, part).start()

            token_copy(2, right, c, part).start()

    for part in range(half_parts):
        forward(1, part)

    grid_rows = block_tokens // GRID_W
    all_rows = table.shape[1] - GRID_W
    later_loads[4].wait()
    is_row = lax.broadcasted_iota(jnp.int32, (GRID_W, half), 1) < half // 2
    for kind, into in enumerate((cosine, sine)):
        by_col = table[kind, all_rows:, :]
        for r in range(grid_rows):
            by_row = table[kind, pl.ds(s * grid_rows + r, 1), :]
            into[r * GRID_W : (r + 1) * GRID_W, :] = jnp.where(is_row, by_row, by_col)

    for k in range(1, chips):
        owner = lax.rem(t + 2 * k, tp_size)
        piece_copy(k, owner).wait_recv()
        piece_across(owner).start()
    for k in range(chips):
        piece_across(lax.rem(twin + 2 * k, tp_size)).wait_recv()
    for i in range(tp_size):
        found = mod_pieces[i]
        mod_rows[0:2, i * piece : (i + 1) * piece] = found[0:2]
        mod_rows[2:4, i * piece : (i + 1) * piece] = 1.0 + found[2:4]
        mod_rows[4:6, i * piece : (i + 1) * piece] = found[4:6]

    flip = jnp.where(2 * z >= chips, 0, 1)
    near = jnp.minimum(z, chips - 1 - z)
    far = jnp.maximum(z, chips - 1 - z)

    def block_of(i):
        r = jnp.maximum(i - (far - near), 0)
        single = i < far - near
        dist = jnp.where(single, far - i, near - lax.div(r, 2))
        turn_of = jnp.where(single, 0, lax.rem(r, 2))
        pick = turn_of + flip - 2 * turn_of * flip
        return z - dist + 2 * dist * pick

    def arrival(i):
        return block_of(chips - 1 - i)

    def swap(i):
        return jnp.where(i < 2, 1 - i, i) if chips > 2 else i

    tiles = width // LANES

    def normalise(ref, start, count, row):
        def group(g, carry):
            place = aligned(start(g), half_rows, ROWS)

            def tile(i):
                return ref[place, i * LANES : (i + 1) * LANES].astype(jnp.float32)

            sums = tile(0)
            for i in range(1, tiles):
                sums = sums + tile(i)
            center = jnp.sum(sums, axis=1, keepdims=True) * (1.0 / width)
            squares = jnp.zeros((half_rows, LANES), jnp.float32)
            for i in range(tiles):
                x = tile(i) - center
                squares = squares + x * x
            spread = jnp.sum(squares, axis=1, keepdims=True) * (1.0 / width)
            inverse = lax.rsqrt(spread + EPSILON)
            for i in range(tiles):
                cols = slice(i * LANES, (i + 1) * LANES)
                x = (tile(i) - center) * inverse
                y = x * mod_rows[2 + row : 3 + row, cols] + mod_rows[row : row + 1, cols]
                normed[aligned(g * half_rows, half_rows, ROWS), cols] = y.astype(jnp.bfloat16)
            return carry

        lax.fori_loop(0, count, group, 0)

    slots = chips + 2
    early = ctx_total + (chips - 1) * sp_size * pair

    def size_of(kind):
        return {"block": pair, "half": rows, "context": ctx_rows}[kind]

    def span_of(kind, slot):
        if kind == "context":
            return 0
        if kind == "block":
            return ctx_total + slot * sp_size * pair
        return early + (slot - (chips - 1)) * sp_size * rows

    def kv_place(kind, slot, owner):
        size = size_of(kind)
        return aligned(span_of(kind, slot) + owner * size, size, ROWS)

    def stage_place(kind, slot):
        if kind == "context":
            return pl.ds(block_tokens, ctx_rows)
        start = slot * pair if kind == "block" else (chips - 1) * pair + (slot - chips + 1) * rows
        return aligned(start, size_of(kind), ROWS)

    def kv_copy(k, owner, kind, slot):
        to = lax.rem(s + k, sp_size)
        return remote(
            kv_stage.at[lax.rem(to, heads), stage_place(kind, slot)],
            keys_values.at[kv_place(kind, slot, owner)],
            kv_send.at[k],
            kv_recv.at[owner, slot],
            sp=to,
        )

    def wanted(k):
        to = lax.rem(s + k, sp_size)
        return lax.div(lax.rem(to, plane), heads) == c

    def twin_copy(owner, kind, slot):
        place = keys_values.at[kv_place(kind, slot, owner)]
        return remote(place, place, kv_twin.at[0], kv_pass.at[slot], tp=twin)

    def twin_all(kind, slot):
        place = keys_values.at[
            aligned(span_of(kind, slot), sp_size * size_of(kind), ROWS)
        ]
        return remote(place, place, kv_twin.at[0], kv_pass.at[slot], tp=twin)

    def hand_out(keys, values, kind, slot):
        place = stage_place(kind, slot)
        for g in range(heads):
            kv_stage[g, place, :head] = keys[:, g * head : (g + 1) * head]
            kv_stage[g, place, head:] = values[:, g * head : (g + 1) * head]
        for k in range(1, sp_size):

            @pl.when(wanted(k))
            def _():
                kv_copy(k, s, kind, slot).start()

        @pl.when(is_owner)
        def _():
            keys_values[kv_place(kind, slot, s), :] = kv_stage[mine, place, :]
            twin_copy(s, kind, slot).start()

    def pass_on(kind, slot):
        @pl.when(is_owner)
        def _():
            for k in range(1, sp_size):
                owner = lax.rem(s + k, sp_size)
                kv_copy(k, owner, kind, slot).wait_recv()
                twin_copy(owner, kind, slot).start()

    def take(kind, slot):
        @pl.when(jnp.logical_not(is_owner))
        def _():
            twin_all(kind, slot).wait_recv()

    def q_copy(g, rel, source, b, start, count):
        core = c + rel - 2 * c * rel
        return remote(
            q_stage.at[g, aligned(b * pair + core * rows + start, count, ROWS)],
            queries.at[b, aligned(source * rows + start, count, ROWS)],
            q_send.at[2 * g + rel],
            q_recv.at[source, b],
            sp=base + c * heads + g,
            tp=twin if rel else t,
        )

    def out_copy(b, k, index):
        to = lax.rem(my_head + k, plane)
        return remote(
            out_stage.at[b, aligned(to * rows, rows, ROWS)],
            attended.at[b, index],
            out_send.at[k],
            out_recv.at[b, index],
            sp=base + to,
        )

    quarter = half // 4

    def turn(raw, cos, sin):
        lane = lax.broadcasted_iota(jnp.int32, cos.shape, 1)
        low = lax.rem(lane, 2 * quarter) < quarter
        found = []
        for i in range(local // half):
            v = raw[:, i * half : (i + 1) * half].astype(jnp.bfloat16).astype(jnp.float32)
            other = jnp.where(low, pltpu.roll(v, half - quarter, 1), pltpu.roll(v, quarter, 1))
            found.append((v * cos + other * sin).astype(jnp.bfloat16))
        return jnp.concatenate(found, axis=1)

    def process(b, kind, slot, start):
        count = rows if kind == "block" else half_rows
        first_part = start // ROWS
        for i in range(count // ROWS):
            token_copy(2, b, 1 - c, first_part + i).wait_recv()
        if kind == "block":
            normalise(tokens, lambda g: b * pair + g * half_rows, 4, 0)
        else:
            normalise(tokens, lambda g: b * pair + g * rows + start, 2, 0)

        def of(ref):
            if kind == "block":
                return ref[aligned(b * pair, pair, ROWS), :]
            return jnp.concatenate(
                [
                    ref[aligned(b * pair + core * rows + start, half_rows, ROWS), :]
                    for core in range(2)
                ],
                axis=0,
            )

        cos, sin = of(cosine), of(sine)
        x = normed[: 2 * count, :]
        hand_out(
            turn(jnp.dot(x, wk[...], preferred_element_type=jnp.float32), cos, sin),
            jnp.dot(x, wv[...], preferred_element_type=jnp.float32).astype(jnp.bfloat16),
            kind,
            slot,
        )
        turned = turn(jnp.dot(x, wq[...], preferred_element_type=jnp.float32), cos, sin)
        for g in range(heads):
            for core in range(2):
                q_stage[g, aligned(b * pair + core * rows + start, count, ROWS), :] = turned[
                    core * count : (core + 1) * count, g * head : (g + 1) * head
                ]
            q_copy(g, 1, my_head, b, start, count).start()

            @pl.when(c * heads + g != my_head)
            def _():
                q_copy(g, 0, my_head, b, start, count).start()

            @pl.when(c * heads + g == my_head)
            def _():
                queries[b, aligned(my_head * rows + start, count, ROWS), :] = q_stage[
                    g, aligned(b * pair + c * rows + start, count, ROWS), :
                ]

    for i in (1, 2, 3):
        later_loads[i].wait()
    normalise(context_tokens, lambda g: g * half_rows, ctx_rows // half_rows, 1)
    hand_out(
        jnp.dot(normed[:ctx_rows, :], wk[...], preferred_element_type=jnp.float32).astype(
            jnp.bfloat16
        ),
        jnp.dot(normed[:ctx_rows, :], wv[...], preferred_element_type=jnp.float32).astype(
            jnp.bfloat16
        ),
        "context",
        slots - 1,
    )
    for part in range(half_parts, parts):
        forward(1, part)
    later_loads[0].wait()
    later_loads[5].wait()

    def forwarded(i):
        dist = jnp.abs(arrival(i) - z)
        ahead = jnp.where(i == 1, half_parts, jnp.where(i == 2, parts - 1, parts))
        return jnp.where(near == 0, dist * parts, jnp.minimum(dist * parts + ahead, far * parts))

    def forward_all(start, stop):
        def one(q, carry):
            forward(1 + lax.div(q, parts), lax.rem(q, parts))
            return carry

        lax.fori_loop(start, stop, one, 0)

    def step(i, done):
        goal = jnp.where(i > 0, jnp.maximum(forwarded(i), done), done)
        forward_all(done, goal)
        process(arrival(i), "block", i, 0)

        @pl.when(i == 0)
        def _():
            pass_on("context", slots - 1)

        @pl.when(i > 0)
        def _():
            pass_on("block", i - 1)

        return goal

    done = lax.fori_loop(0, chips - 1, step, jnp.int32(parts))
    half_way = jnp.maximum(
        done, jnp.where(near == 0, (far - 1) * parts + half_parts, far * parts)
    )
    farthest = arrival(chips - 1)
    forward_all(done, half_way)
    process(farthest, "half", chips - 1, 0)
    pass_on("block", chips - 2)

    tile = plane * rows
    factor = half ** (-0.5) * LOG2E
    head_copy(1 - c).wait_recv()
    later_loads[6].wait()
    weight_of_second = per_head[owner_core, pl.ds(2 * mine, 1), :][:, 0:1]
    raised = per_head[owner_core, pl.ds(2 * mine + 1, 1), :][:, 0:1] * LOG2E

    def partial(b, m, start, stop, lifted):
        scores = (
            lax.dot_general(
                queries[b, :, m * half : (m + 1) * half],
                keys_values[start:stop, m * half : (m + 1) * half],
                (((1,), (1,)), ((), ())),
                preferred_element_type=jnp.float32,
            )
            * factor
        )
        if lifted:
            scores = jnp.concatenate([scores[:, :lifted] + raised, scores[:, lifted:]], axis=1)
        peak = jnp.max(scores, axis=1, keepdims=True)
        weights = jnp.exp2(scores - peak)
        sums = jnp.sum(weights, axis=1, keepdims=True)
        found = jnp.dot(
            weights.astype(jnp.bfloat16),
            keys_values[start:stop, head:],
            preferred_element_type=jnp.float32,
        )
        return peak, sums, found

    def wait_queries(b):
        for k in range(plane):
            source = lax.rem(my_head + k, plane)

            @pl.when(jnp.logical_or(k > 0, jnp.logical_not(is_owner)))
            def _():
                q_copy(0, 0, source, b, 0, rows).wait_recv()

    def begin(b):
        wait_queries(b)
        for m in range(2):
            peak, sums, found = partial(b, m, 0, early, ctx_total)
            held_peak[m] = jnp.broadcast_to(peak, (tile, LANES))
            held_sums[m] = jnp.broadcast_to(sums, (tile, LANES))
            held[m] = found

    def finish(b):
        outs = []
        for m in range(2):
            peak, sums, found = partial(b, m, early, keys_values.shape[0], 0)
            old_peak = held_peak[m][:, 0:1]
            top = jnp.maximum(peak, old_peak)
            now = jnp.exp2(peak - top)
            before = jnp.exp2(old_peak - top)
            sums = sums * now + held_sums[m][:, 0:1] * before
            outs.append((found * now + held[m] * before) / sums)
        hand_back(b, outs)

    def whole(b):
        wait_queries(b)
        outs = []
        for m in range(2):
            _, sums, found = partial(b, m, 0, keys_values.shape[0], ctx_total)
            outs.append(found / sums)
        hand_back(b, outs)

    def hand_back(b, outs):
        diff = outs[0] - weight_of_second * outs[1]
        mean = jnp.sum(diff * diff, axis=1, keepdims=True) * (1.0 / head)
        out_stage[b, :, :] = (diff * lax.rsqrt(mean + EPSILON) * gain[...]).astype(jnp.bfloat16)
        for k in range(1, plane):
            out_copy(b, k, my_head).start()
        attended[b, my_head] = out_stage[b, aligned(my_head * rows, rows, ROWS), :]

    forward_all(half_way, jnp.maximum(half_way, far * parts))
    process(farthest, "half", chips, half_rows)
    pass_on("half", chips - 1)
    take("context", slots - 1)

    def take_block(i, carry):
        take("block", i)
        return carry

    lax.fori_loop(0, chips - 1, take_block, 0)
    begin(block_of(swap(0)))
    pass_on("half", chips)
    take("half", chips - 1)
    take("half", chips)
    finish(block_of(swap(0)))
    weight_copy(1 - c).wait_recv()
    later_loads[7].wait()

    span = width // UNITS
    at_end = (z == 0) | (z + 1 == chips)

    def right_copy(u):
        return remote(stage.at[u], from_left.at[u], stage_sem.at[0], left_sem.at[u], tp=t + 2)

    def left_copy(u):
        return remote(stage.at[u], from_right.at[u], stage_sem.at[0], right_sem.at[u], tp=t - 2)

    def project(b):
        for k in range(1, plane):
            out_copy(b, k, lax.rem(my_head + k, plane)).wait_recv()
        x = jnp.concatenate([attended[b, g] for g in range(plane)], axis=1)
        for n in range(UNITS):
            u = b * UNITS + n
            found = jnp.dot(
                x, weight[:, n * span : (n + 1) * span], preferred_element_type=jnp.float32
            )
            own[u] = found

            @pl.when(at_end & (b != z))
            def _():
                stage[u] = found.astype(jnp.bfloat16)

                @pl.when(z == 0)
                def _():
                    right_copy(u).start()

                @pl.when(z > 0)
                def _():
                    left_copy(u).start()

    def attend_step(i, carry):
        @pl.when(i + 1 < chips)
        def _():
            whole(block_of(swap(i + 1)))

        project(block_of(swap(i)))
        return carry

    lax.fori_loop(0, chips, attend_step, 0)

    def copies_left():
        for k in range(1, plane):
            remote(
                attended.at[:, 0], attended.at[:, 0], out_send.at[k], out_recv.at[0, 0], tp=twin
            ).wait_send()

        def sent_tokens(b, carry):
            place = tokens.at[aligned(b * rows, rows, ROWS)]

            @pl.when((b <= z) & (z + 1 < chips))
            def _():
                remote(place, place, tok_send.at[0, b], tok_recv.at[0], tp=twin).wait_send()

            @pl.when((b >= z) & (z > 0))
            def _():
                remote(place, place, tok_send.at[1, b], tok_recv.at[0], tp=twin).wait_send()

            return carry

        lax.fori_loop(0, chips, sent_tokens, 0)
        place = tokens.at[: chips * rows]
        remote(place, place, tok_send.at[2, 0], tok_recv.at[0], tp=twin).wait_send()
        for g in range(heads):
            place = q_stage.at[g, : chips * rows]
            remote(place, place, q_send.at[2 * g + 1], q_recv.at[0, 0], tp=twin).wait_send()

            @pl.when(c * heads + g != my_head)
            def _():
                remote(place, place, q_send.at[2 * g], q_recv.at[0, 0], tp=twin).wait_send()

        for k in range(1, sp_size):

            @pl.when(wanted(k))
            def _():
                place = kv_stage.at[0]
                remote(place, place, kv_send.at[k], kv_recv.at[0, 0], tp=twin).wait_send()

        @pl.when(is_owner)
        def _():
            remote(
                keys_values, keys_values, kv_twin.at[0], kv_pass.at[0], tp=twin
            ).wait_send()

        place = mod_parts.at[: sp_size - 1]
        remote(place, place, part_send, part_recv.at[0], tp=twin).wait_send()
        place = mod_pieces.at[: tp_size - 1]
        remote(place, place, piece_send, piece_recv.at[0], tp=twin).wait_send()
        head_copy(c).wait_send()
        weight_copy(c).wait_send()

    copies_left()

    hop = 2

    def combine_step(i, carry):
        q = jnp.maximum(i - hop * (chips - 1 - z), 0)
        b = swap(lax.div(q, UNITS))
        u = b * UNITS + lax.rem(q, UNITS)

        @pl.when((i >= hop * (chips - 1 - z)) & (b < z))
        def _():
            left_copy(u).wait_recv()
            stage[u] = (own[u] + from_right[u].astype(jnp.float32)).astype(jnp.bfloat16)
            left_copy(u).start()

        p = jnp.maximum(i - hop * z, 0)
        e = chips - 1 - swap(lax.div(p, UNITS))
        v = e * UNITS + lax.rem(p, UNITS)

        @pl.when((i >= hop * z) & (e > z))
        def _():
            right_copy(v).wait_recv()
            stage[v] = (own[v] + from_left[v].astype(jnp.float32)).astype(jnp.bfloat16)
            right_copy(v).start()

        return carry

    @pl.when(jnp.logical_not(at_end))
    def _():
        lax.fori_loop(0, (chips - 1) * UNITS + hop * (chips - 1), combine_step, 0)

    for n in range(UNITS):
        u = z * UNITS + n
        cols = slice(n * span, (n + 1) * span)

        @pl.when(z > 0)
        def _():
            right_copy(u).wait_recv()
            own[u] = own[u] + from_left[u].astype(jnp.float32)

        @pl.when(z + 1 < chips)
        def _():
            left_copy(u).wait_recv()
            own[u] = own[u] + from_right[u].astype(jnp.float32)

        result[:, cols] = (
            tokens[aligned(t * rows, rows, ROWS), cols].astype(jnp.float32)
            + mod_rows[4:5, cols] * own[u]
        ).astype(jnp.bfloat16)

    place = stage.at[: (chips - 1) * UNITS]
    remote(place, place, stage_sem.at[0], left_sem.at[0], tp=twin).wait_send()


def tables(grid_rows, half):
    quarter = half // 4
    inverse = (ROPE_BASE ** (-np.arange(quarter) / quarter)).astype(np.float32)
    sign = np.where(np.arange(half) % (2 * quarter) < quarter, -1.0, 1.0)
    places = np.concatenate([np.arange(grid_rows), np.arange(GRID_W)]).astype(np.float32)
    angles = (places[:, None] * np.tile(inverse, 4)).astype(np.float64)
    return np.stack([np.cos(angles), np.sin(angles) * sign]).astype(np.float32)


def shards(
    sp_size,
    tp_size,
    latent,
    context,
    condition,
    context_condition,
    modulation,
    query_weight,
    key_weight,
    value_weight,
    lambdas,
    context_lift,
    head_gain,
    output_weight,
):
    rows, width = latent.shape
    chips = tp_size // 2
    local = query_weight.shape[1]
    heads = lambdas.shape[0]
    head = local // heads
    half = head // 2
    plane = 2 * heads
    block_tokens = rows * tp_size
    ctx_rows = context.shape[0]
    piece = modulation.shape[2]
    depth = modulation.shape[1]
    parts = rows // ROWS
    table = tables(sp_size * block_tokens // GRID_W, half)
    vmem = pl.BlockSpec(memory_space=pltpu.VMEM)
    smem = pl.BlockSpec(memory_space=pltpu.SMEM)
    anywhere = pl.BlockSpec(memory_space=pl.ANY)
    bf16, f32 = jnp.bfloat16, jnp.float32
    dma = pltpu.SemaphoreType.DMA
    units = (UNITS * chips, rows, width // UNITS)
    return pl.pallas_call(
        functools.partial(block_kernel, sp_size, tp_size),
        out_shape=jax.ShapeDtypeStruct((rows, width), bf16),
        in_specs=[anywhere] * 9 + [smem] * 2 + [anywhere] * 2,
        out_specs=vmem,
        scratch_shapes=[
            pltpu.VMEM((block_tokens, width), bf16),
            pltpu.VMEM(context.shape, bf16),
            pltpu.VMEM((max(2 * rows, ctx_rows), width), bf16),
            pltpu.VMEM(modulation.shape, bf16),
            pltpu.VMEM((width, local), bf16),
            pltpu.VMEM((width, local), bf16),
            pltpu.VMEM((width, local), bf16),
            pltpu.VMEM((2 * local, width), bf16),
            pltpu.VMEM((sp_size * (ctx_rows + block_tokens), 2 * head), bf16),
            pltpu.VMEM((chips, plane * rows, head), bf16),
            pltpu.VMEM((heads, block_tokens + ctx_rows, 2 * head), bf16),
            pltpu.VMEM((heads, block_tokens, head), bf16),
            pltpu.VMEM((chips, plane * rows, head), bf16),
            pltpu.VMEM((chips, plane, rows, head), bf16),
            pltpu.VMEM(units, f32),
            pltpu.VMEM(units, bf16),
            pltpu.VMEM(units, bf16),
            pltpu.VMEM(units, bf16),
            pltpu.VMEM((sp_size, 8, piece), f32),
            pltpu.VMEM((tp_size, 8, piece), f32),
            pltpu.VMEM((8, width), f32),
            pltpu.VMEM((2, depth), f32),
            pltpu.VMEM(table.shape, f32),
            pltpu.VMEM((block_tokens, half), f32),
            pltpu.VMEM((block_tokens, half), f32),
            pltpu.VMEM((1, head), f32),
            pltpu.VMEM((2, 8, LANES), f32),
            pltpu.VMEM((2, plane * rows, head), f32),
            pltpu.VMEM((2, plane * rows, LANES), f32),
            pltpu.VMEM((2, plane * rows, LANES), f32),
            dma((11,)),
            dma((3, chips)),
            dma((parts * tp_size,)),
            dma(()),
            dma((sp_size,)),
            dma(()),
            dma((tp_size,)),
            dma((sp_size,)),
            dma((1,)),
            dma((sp_size, chips + 2)),
            dma((chips + 2,)),
            dma((2 * heads,)),
            dma((plane, chips)),
            dma((plane,)),
            dma((chips, plane)),
            dma((2,)),
            dma((2,)),
            dma((1,)),
            dma((UNITS * chips,)),
            dma((UNITS * chips,)),
        ],
        compiler_params=pltpu.CompilerParams(
            collective_id=0, has_side_effects=True, vmem_limit_bytes=VMEM_LIMIT
        ),
        name="block",
    )(
        latent,
        context,
        condition.reshape(1, -1),
        context_condition.reshape(1, -1),
        modulation,
        query_weight,
        key_weight,
        value_weight,
        table,
        lambdas,
        context_lift,
        head_gain.reshape(1, -1),
        output_weight,
    )


def solution(mesh):
    in_specs = (
        P(("sp", "tp"), None),
        P("sp", None),
        P(),
        P(),
        P(None, "sp", "tp"),
        P(None, "tp"),
        P(None, "tp"),
        P(None, "tp"),
        P("tp"),
        P("tp"),
        P(),
        P("tp", None),
    )
    out_specs = P(("sp", "tp"), None)
    body = functools.partial(shards, mesh.shape["sp"], mesh.shape["tp"])
    return jax.shard_map(body, mesh=mesh, in_specs=in_specs, out_specs=out_specs, check_vma=False)
```

time: 103 us -> 100 us (0.971)
  Pallas kernels: 100 us -> 97.9 us
    pallas_call x1, Pallas kernels: 100 us -> 97.9 us  [shards(): pl.pallas_call(functools.partial(block_kernel, sp_size, tp_size), out_sha...]
where the time goes in v2:
time: 100 us; the launch traced here: 99.8 us
  Pallas kernels  97.9 us (98%)
  local copies, waits for them, and re-layouts  1.87 us (2%)
    pallas_call x1, Pallas kernels, shards(): pl.pallas_call(functools.partial(block_kernel, sp_size, tp_size), out_sha...  97.9 us

profile of v2, /device:TPU:0, one launch (start us, length us, event | category | flops | bytes accessed | tf_op | source)
XLA Modules:
  0.0 99.8 jit_solution(17478601312571916147)
XLA Ops:
  0.0 97.9 %block.1 = bf16[64,4096]{1,0:T(8,128)(2,1)} custom-call(bf16[64,4096]{1,0:T(8,128)(2,1)} %latent.1, bf16[128,4096]{1,0:T(8,128)(2,1)} %context.1, f32[1,4096]{1,0:T(1,128)} %bitcast.3, f32[1,4096]{1,0:T(1,128)} %bitcast.4, bf16[3,1024,512]{2,1,0:T(8,128)(2,1)} %modulation.1, bf16[4096,512]{1,0:T(8,128)(2,1)} %query_weight.1, bf16[4096,512]{1,0:T(8,128)(2,1)} %key_weight.1, ...), custom_call_target="tpu_custom_call" | custom-call | tf_op jit(solution)/shard_map/block/pallas_call | solution.py:858
  97.9 1.9 %copy.15 = bf16[64,4096]{1,0:T(8,128)(2,1)} copy(bf16[64,4096]{1,0:T(8,128)(2,1)} %block.1) | data formatting | bytes 1048576

commit v3 on v2

--- a/solution.py
+++ b/solution.py
@@ -15,7 +15,7 @@
 ROWS = 16
 LANES = 128
 UNITS = 4
-VMEM_LIMIT = 62 * 1024 * 1024
+VMEM_LIMIT = 53 * 1024 * 1024
 MESH = pl.DeviceIdType.MESH
 
 
@@ -78,6 +78,7 @@
     sine,
     gain,
     per_head,
+    scalars,
     held,
     held_peak,
     held_sums,
@@ -117,8 +118,8 @@
     ctx_rows = context.shape[0]
     ctx_total = ctx_rows * sp_size
     local = query_weight.shape[1]
-    heads = lambdas.shape[0]
-    head = local // heads
+    head = gain_in.shape[1]
+    heads = local // head
     half = head // 2
     plane = 2 * heads
     piece = modulation.shape[2]
@@ -140,6 +141,8 @@
         load(0, condition.at[:, here], vectors_in.at[0:1]),
         load(1, context_condition.at[:, here], vectors_in.at[1:2]),
         load(2, modulation, mod_weight),
+        load(11, lambdas, scalars.at[0]),
+        load(12, lift, scalars.at[1]),
     ]
     later_loads = [
         load(3, latent, own_slot),
@@ -166,9 +169,6 @@
             )
     for copy in first_loads + later_loads[:-1]:
         copy.start()
-    for g in range(heads):
-        per_head[c, 2 * g : 2 * g + 1, :] = jnp.full((1, LANES), lambdas[g], jnp.float32)
-        per_head[c, 2 * g + 1 : 2 * g + 2, :] = jnp.full((1, LANES), lift[g], jnp.float32)
     pl.semaphore_wait(barrier, tp_size - 1 + 2 * (sp_size - 1))
 
     def token_copy(kind, b, core, part, mine_first=False):
@@ -207,6 +207,13 @@
         jnp.broadcast_to(v[0:1], (ROWS, depth)),
         jnp.broadcast_to(v[1:2], (ROWS, depth)),
     ).astype(jnp.bfloat16)
+    first_loads[3].wait()
+    first_loads[4].wait()
+    for i in range(2):
+        for g in range(heads):
+            per_head[c, 2 * g + i : 2 * g + i + 1, :] = jnp.broadcast_to(
+                scalars[i][:, g : g + 1], (1, LANES)
+            )
     first_loads[2].wait()
     for r in range(3):
         found = jnp.dot(vectors, mod_weight[r], preferred_element_type=jnp.float32)
@@ -366,6 +373,7 @@
 
     slots = chips + 2
     early = ctx_total + (chips - 1) * sp_size * pair
+    most = early + sp_size * rows
 
     def size_of(kind):
         return {"block": pair, "half": rows, "context": ctx_rows}[kind]
@@ -614,7 +622,7 @@
     def begin(b):
         wait_queries(b)
         for m in range(2):
-            peak, sums, found = partial(b, m, 0, early, ctx_total)
+            peak, sums, found = partial(b, m, 0, most, ctx_total)
             held_peak[m] = jnp.broadcast_to(peak, (tile, LANES))
             held_sums[m] = jnp.broadcast_to(sums, (tile, LANES))
             held[m] = found
@@ -622,7 +630,7 @@
     def finish(b):
         outs = []
         for m in range(2):
-            peak, sums, found = partial(b, m, early, keys_values.shape[0], 0)
+            peak, sums, found = partial(b, m, most, keys_values.shape[0], 0)
             old_peak = held_peak[m][:, 0:1]
             top = jnp.maximum(peak, old_peak)
             now = jnp.exp2(peak - top)
@@ -657,9 +665,9 @@
         return carry
 
     lax.fori_loop(0, chips - 1, take_block, 0)
+    take("half", chips - 1)
     begin(block_of(swap(0)))
     pass_on("half", chips)
-    take("half", chips - 1)
     take("half", chips)
     finish(block_of(swap(0)))
     weight_copy(1 - c).wait_recv()
@@ -697,15 +705,62 @@
                 def _():
                     left_copy(u).start()
 
-    def attend_step(i, carry):
-        @pl.when(i + 1 < chips)
-        def _():
-            whole(block_of(swap(i + 1)))
-
-        project(block_of(swap(i)))
+    hop = 2
+
+    def combine_step(i, carry):
+        q = jnp.maximum(i - hop * (chips - 1 - z), 0)
+        b = swap(lax.div(q, UNITS))
+        u = b * UNITS + lax.rem(q, UNITS)
+
+        @pl.when((i >= hop * (chips - 1 - z)) & (b < z))
+        def _():
+            left_copy(u).wait_recv()
+            stage[u] = (own[u] + from_right[u].astype(jnp.float32)).astype(jnp.bfloat16)
+            left_copy(u).start()
+
+        p = jnp.maximum(i - hop * z, 0)
+        e = chips - 1 - swap(lax.div(p, UNITS))
+        v = e * UNITS + lax.rem(p, UNITS)
+
+        @pl.when((i >= hop * z) & (e > z))
+        def _():
+            right_copy(v).wait_recv()
+            stage[v] = (own[v] + from_left[v].astype(jnp.float32)).astype(jnp.bfloat16)
+            right_copy(v).start()
+
         return carry
 
-    lax.fori_loop(0, chips, attend_step, 0)
+    def combine(start, stop):
+        @pl.when(jnp.logical_not(at_end))
+        def _():
+            lax.fori_loop(start, stop, combine_step, 0)
+
+    steps = 2 * chips - 1
+
+    def attend_step(k, carry):
+        index = lax.div(k, 2)
+        odd = lax.rem(k, 2) == 1
+        attends = jnp.where(at_end, odd, jnp.logical_not(odd) & (k + 1 < steps))
+
+        @pl.when(attends)
+        def _():
+            whole(block_of(swap(index + 1)))
+
+        @pl.when(jnp.logical_not(attends))
+        def _():
+            project(block_of(swap(index)))
+
+        @pl.when(k == steps - 3)
+        def _():
+            combine(0, hop + 1)
+
+        @pl.when(k == steps - 2)
+        def _():
+            combine(hop + 1, hop + 2)
+
+        return carry
+
+    lax.fori_loop(0, steps, attend_step, 0)
 
     def copies_left():
         for k in range(1, plane):
@@ -758,35 +813,7 @@
         weight_copy(c).wait_send()
 
     copies_left()
-
-    hop = 2
-
-    def combine_step(i, carry):
-        q = jnp.maximum(i - hop * (chips - 1 - z), 0)
-        b = swap(lax.div(q, UNITS))
-        u = b * UNITS + lax.rem(q, UNITS)
-
-        @pl.when((i >= hop * (chips - 1 - z)) & (b < z))
-        def _():
-            left_copy(u).wait_recv()
-            stage[u] = (own[u] + from_right[u].astype(jnp.float32)).astype(jnp.bfloat16)
-            left_copy(u).start()
-
-        p = jnp.maximum(i - hop * z, 0)
-        e = chips - 1 - swap(lax.div(p, UNITS))
-        v = e * UNITS + lax.rem(p, UNITS)
-
-        @pl.when((i >= hop * z) & (e > z))
-        def _():
-            right_copy(v).wait_recv()
-            stage[v] = (own[v] + from_left[v].astype(jnp.float32)).astype(jnp.bfloat16)
-            right_copy(v).start()
-
-        return carry
-
-    @pl.when(jnp.logical_not(at_end))
-    def _():
-        lax.fori_loop(0, (chips - 1) * UNITS + hop * (chips - 1), combine_step, 0)
+    combine(hop + 2, (chips - 1) * (UNITS + hop))
 
     for n in range(UNITS):
         u = z * UNITS + n
@@ -818,6 +845,10 @@
     places = np.concatenate([np.arange(grid_rows), np.arange(GRID_W)]).astype(np.float32)
     angles = (places[:, None] * np.tile(inverse, 4)).astype(np.float64)
     return np.stack([np.cos(angles), np.sin(angles) * sign]).astype(np.float32)
+
+
+def row(x):
+    return x.reshape(1, -1) if x.size > 1 else jnp.broadcast_to(x.reshape(1, 1), (1, LANES))
 
 
 def shards(
@@ -850,15 +881,14 @@
     parts = rows // ROWS
     table = tables(sp_size * block_tokens // GRID_W, half)
     vmem = pl.BlockSpec(memory_space=pltpu.VMEM)
-    smem = pl.BlockSpec(memory_space=pltpu.SMEM)
-    anywhere = pl.BlockSpec(memory_space=pl.ANY)
+    anywhere = pl.BlockSpec(memory_space=pltpu.HBM)
     bf16, f32 = jnp.bfloat16, jnp.float32
     dma = pltpu.SemaphoreType.DMA
     units = (UNITS * chips, rows, width // UNITS)
     return pl.pallas_call(
         functools.partial(block_kernel, sp_size, tp_size),
         out_shape=jax.ShapeDtypeStruct((rows, width), bf16),
-        in_specs=[anywhere] * 9 + [smem] * 2 + [anywhere] * 2,
+        in_specs=[anywhere] * 13,
         out_specs=vmem,
         scratch_shapes=[
             pltpu.VMEM((block_tokens, width), bf16),
@@ -888,10 +918,11 @@
             pltpu.VMEM((block_tokens, half), f32),
             pltpu.VMEM((1, head), f32),
             pltpu.VMEM((2, 8, LANES), f32),
+            pltpu.VMEM((2,) + row(lambdas).shape, f32),
             pltpu.VMEM((2, plane * rows, head), f32),
             pltpu.VMEM((2, plane * rows, LANES), f32),
             pltpu.VMEM((2, plane * rows, LANES), f32),
-            dma((11,)),
+            dma((13,)),
             dma((3, chips)),
             dma((parts * tp_size,)),
             dma(()),
@@ -917,19 +948,24 @@
         ),
         name="block",
     )(
-        latent,
-        context,
-        condition.reshape(1, -1),
-        context_condition.reshape(1, -1),
-        modulation,
-        query_weight,
-        key_weight,
-        value_weight,
-        table,
-        lambdas,
-        context_lift,
-        head_gain.reshape(1, -1),
-        output_weight,
+        *(
+            pltpu.with_memory_space_constraint(x, pltpu.HBM)
+            for x in (
+                latent,
+                context,
+                row(condition),
+                row(context_condition),
+                modulation,
+                query_weight,
+                key_weight,
+                value_weight,
+                table,
+                row(lambdas),
+                row(context_lift),
+                row(head_gain),
+                output_weight,
+            )
+        )
     )
 
 

time: 100 us -> 92.7 us (0.927)
  Pallas kernels: 97.9 us -> 91.8 us
  local copies, waits for them, and re-layouts: 1.87 us -> 0.8 us
    pallas_call x1, Pallas kernels: 97.9 us -> 91.8 us  [shards(): pl.pallas_call(functools.partial(block_kernel, sp_size, tp_size), out_sha...]
    unnamed x1, local copies, waits for them, and re-layouts: 1.87 us -> 0.8 us
where the time goes in v3:
time: 92.7 us; the launch traced here: 92.6 us
  Pallas kernels  91.8 us (99%)
    pallas_call x1, Pallas kernels, shards(): pl.pallas_call(functools.partial(block_kernel, sp_size, tp_size), out_sha...  91.8 us

profile of v3, /device:TPU:0, one launch (start us, length us, event | category | flops | bytes accessed | tf_op | source)
XLA Modules:
  0.0 92.6 jit_solution(14038743267499856750)
XLA Ops:
  0.0 91.8 %block.1 = bf16[64,4096]{1,0:T(8,128)(2,1)S(1)} custom-call(bf16[64,4096]{1,0:T(8,128)(2,1)} %latent.1, bf16[128,4096]{1,0:T(8,128)(2,1)} %context.1, f32[1,4096]{1,0:T(1,128)} %bitcast.5, f32[1,4096]{1,0:T(1,128)} %bitcast.6, bf16[3,1024,512]{2,1,0:T(8,128)(2,1)} %modulation.1, bf16[4096,512]{1,0:T(8,128)(2,1)} %query_weight.1, ...), custom_call_target="tpu_custom_call" | custom-call | tf_op jit(solution)/shard_map/block/pallas_call | solution.py:888
  91.8 0.8 copy.15

commit v4 on v3

--- a/solution.py
+++ b/solution.py
@@ -67,8 +67,8 @@
     attended,
     own,
     stage,
-    from_left,
-    from_right,
+    incoming,
+    lent_blocks,
     mod_parts,
     mod_pieces,
     mod_rows,
@@ -102,6 +102,9 @@
     stage_sem,
     left_sem,
     right_sem,
+    lend_send,
+    lend_recv,
+    block_recv,
 ):
     s = lax.axis_index("sp")
     t = lax.axis_index("tp")
@@ -140,7 +143,10 @@
     first_loads = [
         load(0, condition.at[:, here], vectors_in.at[0:1]),
         load(1, context_condition.at[:, here], vectors_in.at[1:2]),
-        load(2, modulation, mod_weight),
+        *(
+            load(i, modulation.at[r], mod_weight.at[:depth, r * piece : (r + 1) * piece])
+            for r, i in enumerate((2, 13, 14))
+        ),
         load(11, lambdas, scalars.at[0]),
         load(12, lift, scalars.at[1]),
     ]
@@ -207,16 +213,21 @@
         jnp.broadcast_to(v[0:1], (ROWS, depth)),
         jnp.broadcast_to(v[1:2], (ROWS, depth)),
     ).astype(jnp.bfloat16)
-    first_loads[3].wait()
-    first_loads[4].wait()
+    first_loads[5].wait()
+    first_loads[6].wait()
     for i in range(2):
         for g in range(heads):
             per_head[c, 2 * g + i : 2 * g + i + 1, :] = jnp.broadcast_to(
                 scalars[i][:, g : g + 1], (1, LANES)
             )
-    first_loads[2].wait()
     for r in range(3):
-        found = jnp.dot(vectors, mod_weight[r], preferred_element_type=jnp.float32)
+        first_loads[2 + r].wait()
+    for r in range(3):
+        found = jnp.dot(
+            vectors,
+            mod_weight[:depth, r * piece : (r + 1) * piece],
+            preferred_element_type=jnp.float32,
+        )
         mod_parts[s, 2 * r : 2 * r + 2, :] = found[0:2]
     mod_parts[s, 6:8, :] = jnp.zeros((2, piece), jnp.float32)
 
@@ -319,6 +330,31 @@
         piece_across(owner).start()
     for k in range(chips):
         piece_across(lax.rem(twin + 2 * k, tp_size)).wait_recv()
+
+    at_end = (z == 0) | (z + 1 == chips)
+    by_end = (z == 1) | (z + 2 == chips)
+    inward = jnp.where(z == 0, t + 2, t - 2)
+    kept = kept_of(width)
+
+    def lent(core):
+        return mod_weight.at[aligned(core * local, local, ROWS), : width - kept]
+
+    lend = remote(
+        output_weight.at[:, kept:], lent(c), lend_send.at[0], lend_recv.at[c], tp=inward
+    )
+
+    def lend_across(core):
+        return remote(lent(core), lent(core), lend_send.at[1], lend_recv.at[core], tp=twin)
+
+    def lend_block(b):
+        return remote(
+            attended.at[b], lent_blocks.at[b], lend_send.at[2], block_recv.at[b], tp=inward
+        )
+
+    @pl.when(at_end)
+    def _():
+        lend.start()
+
     for i in range(tp_size):
         found = mod_pieces[i]
         mod_rows[0:2, i * piece : (i + 1) * piece] = found[0:2]
@@ -395,11 +431,12 @@
         start = slot * pair if kind == "block" else (chips - 1) * pair + (slot - chips + 1) * rows
         return aligned(start, size_of(kind), ROWS)
 
-    def kv_copy(k, owner, kind, slot):
+    def kv_copy(k, owner, kind, slot, first=0, last=2):
+        cols = pl.ds(first * head, (last - first) * head)
         to = lax.rem(s + k, sp_size)
         return remote(
-            kv_stage.at[lax.rem(to, heads), stage_place(kind, slot)],
-            keys_values.at[kv_place(kind, slot, owner)],
+            kv_stage.at[lax.rem(to, heads), stage_place(kind, slot), cols],
+            keys_values.at[kv_place(kind, slot, owner), cols],
             kv_send.at[k],
             kv_recv.at[owner, slot],
             sp=to,
@@ -419,16 +456,24 @@
         ]
         return remote(place, place, kv_twin.at[0], kv_pass.at[slot], tp=twin)
 
-    def hand_out(keys, values, kind, slot):
+    def send_kv(kind, slot, first, last):
+        for k in range(1, sp_size):
+
+            @pl.when(wanted(k))
+            def _():
+                kv_copy(k, s, kind, slot, first, last).start()
+
+    def hand_out(find_keys, find_values, kind, slot):
         place = stage_place(kind, slot)
+        keys = find_keys()
         for g in range(heads):
             kv_stage[g, place, :head] = keys[:, g * head : (g + 1) * head]
+        if kind == "half":
+            send_kv(kind, slot, 0, 1)
+        values = find_values()
+        for g in range(heads):
             kv_stage[g, place, head:] = values[:, g * head : (g + 1) * head]
-        for k in range(1, sp_size):
-
-            @pl.when(wanted(k))
-            def _():
-                kv_copy(k, s, kind, slot).start()
+        send_kv(kind, slot, 1 if kind == "half" else 0, 2)
 
         @pl.when(is_owner)
         def _():
@@ -505,8 +550,8 @@
         cos, sin = of(cosine), of(sine)
         x = normed[: 2 * count, :]
         hand_out(
-            turn(jnp.dot(x, wk[...], preferred_element_type=jnp.float32), cos, sin),
-            jnp.dot(x, wv[...], preferred_element_type=jnp.float32).astype(jnp.bfloat16),
+            lambda: turn(jnp.dot(x, wk[...], preferred_element_type=jnp.float32), cos, sin),
+            lambda: jnp.dot(x, wv[...], preferred_element_type=jnp.float32).astype(jnp.bfloat16),
             kind,
             slot,
         )
@@ -532,12 +577,12 @@
         later_loads[i].wait()
     normalise(context_tokens, lambda g: g * half_rows, ctx_rows // half_rows, 1)
     hand_out(
-        jnp.dot(normed[:ctx_rows, :], wk[...], preferred_element_type=jnp.float32).astype(
-            jnp.bfloat16
-        ),
-        jnp.dot(normed[:ctx_rows, :], wv[...], preferred_element_type=jnp.float32).astype(
-            jnp.bfloat16
-        ),
+        lambda: jnp.dot(
+            normed[:ctx_rows, :], wk[...], preferred_element_type=jnp.float32
+        ).astype(jnp.bfloat16),
+        lambda: jnp.dot(
+            normed[:ctx_rows, :], wv[...], preferred_element_type=jnp.float32
+        ).astype(jnp.bfloat16),
         "context",
         slots - 1,
     )
@@ -673,61 +718,143 @@
     weight_copy(1 - c).wait_recv()
     later_loads[7].wait()
 
-    span = width // UNITS
-    at_end = (z == 0) | (z + 1 == chips)
-
-    def right_copy(u):
-        return remote(stage.at[u], from_left.at[u], stage_sem.at[0], left_sem.at[u], tp=t + 2)
-
-    def left_copy(u):
-        return remote(stage.at[u], from_right.at[u], stage_sem.at[0], right_sem.at[u], tp=t - 2)
-
-    def project(b):
+    sizes = (kept // 2, (width - kept) // 2)
+
+    def columns(kind, n):
+        start = n * sizes[0] if kind == 0 else kept + (n - 2) * sizes[1]
+        return aligned(start, sizes[kind], LANES)
+
+    def right_copy(b, kind, n):
+        cols = columns(kind, n)
+        return remote(
+            stage.at[b, :, cols],
+            incoming.at[b + 1, :, cols],
+            stage_sem.at[0],
+            left_sem.at[b * UNITS + n],
+            tp=t + 2,
+        )
+
+    def left_copy(b, kind, n):
+        cols = columns(kind, n)
+        return remote(
+            stage.at[b, :, cols],
+            incoming.at[b, :, cols],
+            stage_sem.at[0],
+            right_sem.at[b * UNITS + n],
+            tp=t - 2,
+        )
+
+    def rows_of(ref, b):
+        return jnp.concatenate([ref[b, g] for g in range(plane)], axis=1)
+
+    def borrowed(b, n):
+        if isinstance(n, int):
+            if n == 2:
+                lend_block(b).wait_recv()
+        else:
+
+            @pl.when(n == 2)
+            def _():
+                lend_block(b).wait_recv()
+
+        return jnp.dot(
+            rows_of(lent_blocks, b),
+            mod_weight[: 2 * local, aligned((n - 2) * sizes[1], sizes[1], LANES)],
+            preferred_element_type=jnp.float32,
+        )
+
+    def unit_at(q):
+        index, n = lax.div(q, UNITS), lax.rem(q, UNITS)
+        n = jnp.where(n == 0, 2, jnp.where(n == 3, 3, n - 1))
+        for place, (i, piece_of) in enumerate(
+            [(0, 0), (0, 2), (1, 2), (1, 0), (1, 1), (1, 3), (0, 1), (0, 3)]
+        ):
+            index = jnp.where(q == place, i, index)
+            n = jnp.where(q == place, piece_of, n)
+        return swap(index), n
+
+    def send_sums(b, n):
+        @pl.when(z == 0)
+        def _():
+            right_copy(b, 0, n).start()
+
+        @pl.when(z > 0)
+        def _():
+            left_copy(b, 0, n).start()
+
+    def project(i):
+        b = block_of(swap(i))
         for k in range(1, plane):
             out_copy(b, k, lax.rem(my_head + k, plane)).wait_recv()
-        x = jnp.concatenate([attended[b, g] for g in range(plane)], axis=1)
+        sends = at_end & (b != z)
+
+        @pl.when(sends)
+        def _():
+            lend_block(b).start()
+
+        x = rows_of(attended, b)
         for n in range(UNITS):
-            u = b * UNITS + n
-            found = jnp.dot(
-                x, weight[:, n * span : (n + 1) * span], preferred_element_type=jnp.float32
-            )
-            own[u] = found
-
-            @pl.when(at_end & (b != z))
-            def _():
-                stage[u] = found.astype(jnp.bfloat16)
-
-                @pl.when(z == 0)
+            kind = n // 2
+            start = n * sizes[0] if kind == 0 else kept + (n - 2) * sizes[1]
+            cols = slice(start, start + sizes[kind])
+
+            def find():
+                return jnp.dot(x, weight[:, cols], preferred_element_type=jnp.float32)
+
+            if kind == 0:
+                found = find()
+                own[b, :, cols] = found
+
+                @pl.when(sends)
                 def _():
-                    right_copy(u).start()
-
-                @pl.when(z > 0)
+                    stage[b, :, cols] = found.astype(jnp.bfloat16)
+
+                    @pl.when((i > 0) | (n == 0))
+                    def _():
+                        send_sums(b, n)
+            else:
+
+                @pl.when(jnp.logical_not(sends))
                 def _():
-                    left_copy(u).start()
+                    own[b, :, cols] = find()
+
+        @pl.when(at_end & (i == 1))
+        def _():
+            send_sums(block_of(swap(0)), 1)
 
     hop = 2
+
+    def combine_one(b, n, wanted_here, copy, slot, neighbour):
+        for kind in range(2):
+            cols = columns(kind, n)
+            here = wanted_here & (lax.div(n, 2) == kind)
+            received = here & jnp.logical_not(neighbour) if kind else here
+
+            @pl.when(received)
+            def _():
+                copy(b, kind, n).wait_recv()
+                stage[b, :, cols] = (
+                    own[b, :, cols] + incoming[slot, :, cols].astype(jnp.float32)
+                ).astype(jnp.bfloat16)
+                copy(b, kind, n).start()
+
+            if kind:
+
+                @pl.when(here & neighbour)
+                def _():
+                    stage[b, :, cols] = (own[b, :, cols] + borrowed(b, n)).astype(jnp.bfloat16)
+                    copy(b, kind, n).start()
 
     def combine_step(i, carry):
         q = jnp.maximum(i - hop * (chips - 1 - z), 0)
-        b = swap(lax.div(q, UNITS))
-        u = b * UNITS + lax.rem(q, UNITS)
-
-        @pl.when((i >= hop * (chips - 1 - z)) & (b < z))
-        def _():
-            left_copy(u).wait_recv()
-            stage[u] = (own[u] + from_right[u].astype(jnp.float32)).astype(jnp.bfloat16)
-            left_copy(u).start()
-
+        b, n = unit_at(q)
+        here = (i >= hop * (chips - 1 - z)) & (b < z)
+        combine_one(b, n, here, left_copy, b, z + 2 == chips)
         p = jnp.maximum(i - hop * z, 0)
-        e = chips - 1 - swap(lax.div(p, UNITS))
-        v = e * UNITS + lax.rem(p, UNITS)
-
-        @pl.when((i >= hop * z) & (e > z))
-        def _():
-            right_copy(v).wait_recv()
-            stage[v] = (own[v] + from_left[v].astype(jnp.float32)).astype(jnp.bfloat16)
-            right_copy(v).start()
-
+        e, n = unit_at(p)
+        e = chips - 1 - e
+        here = (i >= hop * z) & (e > z)
+        combine_one(e, n, here, right_copy, e + 1, z == 1)
         return carry
 
     def combine(start, stop):
@@ -739,8 +866,7 @@
 
     def attend_step(k, carry):
         index = lax.div(k, 2)
-        odd = lax.rem(k, 2) == 1
-        attends = jnp.where(at_end, odd, jnp.logical_not(odd) & (k + 1 < steps))
+        attends = (lax.rem(k, 2) == 0) & (k + 1 < steps)
 
         @pl.when(attends)
         def _():
@@ -748,11 +874,20 @@
 
         @pl.when(jnp.logical_not(attends))
         def _():
-            project(block_of(swap(index)))
+            project(index)
+
+        @pl.when((k == 3) & by_end)
+        def _():
+            lend.wait_recv()
+            lend_across(c).start()
 
         @pl.when(k == steps - 3)
         def _():
             combine(0, hop + 1)
+
+        @pl.when((k == steps - 2) & by_end)
+        def _():
+            lend_across(1 - c).wait_recv()
 
         @pl.when(k == steps - 2)
         def _():
@@ -816,26 +951,51 @@
     combine(hop + 2, (chips - 1) * (UNITS + hop))
 
     for n in range(UNITS):
-        u = z * UNITS + n
-        cols = slice(n * span, (n + 1) * span)
-
-        @pl.when(z > 0)
-        def _():
-            right_copy(u).wait_recv()
-            own[u] = own[u] + from_left[u].astype(jnp.float32)
-
-        @pl.when(z + 1 < chips)
-        def _():
-            left_copy(u).wait_recv()
-            own[u] = own[u] + from_right[u].astype(jnp.float32)
-
+        kind = n // 2
+        start = n * sizes[0] if kind == 0 else kept + (n - 2) * sizes[1]
+        cols = slice(start, start + sizes[kind])
+
+        def add(copy, slot, present, neighbour):
+            received = present & jnp.logical_not(neighbour) if kind else present
+
+            @pl.when(received)
+            def _():
+                copy(z, kind, n).wait_recv()
+                own[z, :, cols] = own[z, :, cols] + incoming[slot, :, cols].astype(jnp.float32)
+
+            if kind:
+
+                @pl.when(neighbour)
+                def _():
+                    own[z, :, cols] = own[z, :, cols] + borrowed(z, n)
+
+        add(right_copy, z + 1, z > 0, z == 1)
+        add(left_copy, z, z + 1 < chips, z + 2 == chips)
         result[:, cols] = (
             tokens[aligned(t * rows, rows, ROWS), cols].astype(jnp.float32)
-            + mod_rows[4:5, cols] * own[u]
+            + mod_rows[4:5, cols] * own[z, :, cols]
         ).astype(jnp.bfloat16)
 
-    place = stage.at[: (chips - 1) * UNITS]
-    remote(place, place, stage_sem.at[0], left_sem.at[0], tp=twin).wait_send()
+    @pl.when(at_end)
+    def _():
+        place = stage.at[: chips - 1, :, :kept]
+        remote(place, place, stage_sem.at[0], left_sem.at[0], tp=twin).wait_send()
+        lend.wait_send()
+        place = attended.at[: chips - 1]
+        remote(place, place, lend_send.at[2], block_recv.at[0], tp=twin).wait_send()
+
+    @pl.when(jnp.logical_not(at_end))
+    def _():
+        place = stage.at[: chips - 1]
+        remote(place, place, stage_sem.at[0], left_sem.at[0], tp=twin).wait_send()
+
+    @pl.when(by_end)
+    def _():
+        lend_across(c).wait_send()
+
+
+def kept_of(width):
+    return width * 5 // 8
 
 
 def tables(grid_rows, half):
@@ -884,7 +1044,7 @@
     anywhere = pl.BlockSpec(memory_space=pltpu.HBM)
     bf16, f32 = jnp.bfloat16, jnp.float32
     dma = pltpu.SemaphoreType.DMA
-    units = (UNITS * chips, rows, width // UNITS)
+    blocks = (chips, rows, width)
     return pl.pallas_call(
         functools.partial(block_kernel, sp_size, tp_size),
         out_shape=jax.ShapeDtypeStruct((rows, width), bf16),
@@ -894,7 +1054,7 @@
             pltpu.VMEM((block_tokens, width), bf16),
             pltpu.VMEM(context.shape, bf16),
             pltpu.VMEM((max(2 * rows, ctx_rows), width), bf16),
-            pltpu.VMEM(modulation.shape, bf16),
+            pltpu.VMEM((max(depth, 2 * local), max(3 * piece, width - kept_of(width))), bf16),
             pltpu.VMEM((width, local), bf16),
             pltpu.VMEM((width, local), bf16),
             pltpu.VMEM((width, local), bf16),
@@ -905,10 +1065,10 @@
             pltpu.VMEM((heads, block_tokens, head), bf16),
             pltpu.VMEM((chips, plane * rows, head), bf16),
             pltpu.VMEM((chips, plane, rows, head), bf16),
-            pltpu.VMEM(units, f32),
-            pltpu.VMEM(units, bf16),
-            pltpu.VMEM(units, bf16),
-            pltpu.VMEM(units, bf16),
+            pltpu.VMEM(blocks, f32),
+            pltpu.VMEM(blocks, bf16),
+            pltpu.VMEM((chips + 1, rows, width), bf16),
+            pltpu.VMEM((chips, plane, rows, head), bf16),
             pltpu.VMEM((sp_size, 8, piece), f32),
             pltpu.VMEM((tp_size, 8, piece), f32),
             pltpu.VMEM((8, width), f32),
@@ -922,7 +1082,7 @@
             pltpu.VMEM((2, plane * rows, head), f32),
             pltpu.VMEM((2, plane * rows, LANES), f32),
             pltpu.VMEM((2, plane * rows, LANES), f32),
-            dma((13,)),
+            dma((15,)),
             dma((3, chips)),
             dma((parts * tp_size,)),
             dma(()),
@@ -942,6 +1102,9 @@
             dma((1,)),
             dma((UNITS * chips,)),
             dma((UNITS * chips,)),
+            dma((3,)),
+            dma((2,)),
+            dma((chips,)),
         ],
         compiler_params=pltpu.CompilerParams(
             collective_id=0, has_side_effects=True, vmem_limit_bytes=VMEM_LIMIT

time: 92.7 us -> 90.2 us (0.973)
  Pallas kernels: 91.8 us -> 89.2 us
    pallas_call x1, Pallas kernels: 91.8 us -> 89.2 us  [shards(): pl.pallas_call(functools.partial(block_kernel, sp_size, tp_size), out_sha...]
where the time goes in v4:
time: 90.2 us; the launch traced here: 90 us
  Pallas kernels  89.2 us (99%)
    pallas_call x1, Pallas kernels, shards(): pl.pallas_call(functools.partial(block_kernel, sp_size, tp_size), out_sha...  89.2 us

profile of v4, /device:TPU:0, one launch (start us, length us, event | category | flops | bytes accessed | tf_op | source)
XLA Modules:
  0.0 90.0 jit_solution(2352147098151305716)
XLA Ops:
  0.0 89.2 %block.1 = bf16[64,4096]{1,0:T(8,128)(2,1)S(1)} custom-call(bf16[64,4096]{1,0:T(8,128)(2,1)} %latent.1, bf16[128,4096]{1,0:T(8,128)(2,1)} %context.1, f32[1,4096]{1,0:T(1,128)} %bitcast.5, f32[1,4096]{1,0:T(1,128)} %bitcast.6, bf16[3,1024,512]{2,1,0:T(8,128)(2,1)} %modulation.1, bf16[4096,512]{1,0:T(8,128)(2,1)} %query_weight.1, ...), custom_call_target="tpu_custom_call" | custom-call | tf_op jit(solution)/shard_map/block/pallas_call | solution.py:1048
  89.2 0.8 copy.15

commit v5 on v4

--- a/solution.py
+++ b/solution.py
@@ -85,6 +85,7 @@
     local_sem,
     tok_send,
     tok_recv,
+    twin_recv,
     part_send,
     part_recv,
     piece_send,
@@ -100,8 +101,7 @@
     wo_sem,
     head_sem,
     stage_sem,
-    left_sem,
-    right_sem,
+    sums_sem,
     lend_send,
     lend_recv,
     block_recv,
@@ -185,7 +185,7 @@
             latent.at[aligned(part * ROWS, ROWS, ROWS)] if mine_first else place,
             place,
             tok_send.at[kind, 0 if kind == 2 else b],
-            tok_recv.at[parts * slot + part],
+            twin_recv.at[2 * b + lax.div(part, half_parts)] if kind == 2 else tok_recv.at[parts * b + part],
             tp=to,
         )
 
@@ -236,7 +236,7 @@
             mod_parts.at[owner],
             mod_parts.at[owner],
             part_send,
-            part_recv.at[owner],
+            part_recv,
             sp=lax.rem(s + k, sp_size),
         )
 
@@ -273,8 +273,8 @@
     for k in range(1, sp_size):
         part_copy(k, s).start()
     head_copy(c).start()
-    for k in range(1, sp_size):
-        part_copy(k, lax.rem(s + k, sp_size)).wait_recv()
+    place = mod_parts.at[: sp_size - 1]
+    remote(place, place, part_send, part_recv, tp=twin).wait_recv()
     total = mod_parts[0]
     for i in range(1, sp_size):
         total = total + mod_parts[i]
@@ -293,7 +293,7 @@
 
         @pl.when(left >= 0)
         def _():
-            token_copy(2, left, c, part).wait_recv()
+            token_copy(0, left, c, part).wait_recv()
 
             @pl.when(z + 1 < chips)
             def _():
@@ -303,7 +303,7 @@
 
         @pl.when(right < chips)
         def _():
-            token_copy(2, right, c, part).wait_recv()
+            token_copy(1, right, c, part).wait_recv()
 
             @pl.when(z > 0)
             def _():
@@ -438,7 +438,7 @@
             kv_stage.at[lax.rem(to, heads), stage_place(kind, slot), cols],
             keys_values.at[kv_place(kind, slot, owner), cols],
             kv_send.at[k],
-            kv_recv.at[owner, slot],
+            kv_recv.at[slot],
             sp=to,
         )
 
@@ -483,10 +483,10 @@
     def pass_on(kind, slot):
         @pl.when(is_owner)
         def _():
+            place = keys_values.at[: (sp_size - 1) * size_of(kind)]
+            remote(place, place, kv_send.at[0], kv_recv.at[slot], tp=twin).wait_recv()
             for k in range(1, sp_size):
-                owner = lax.rem(s + k, sp_size)
-                kv_copy(k, owner, kind, slot).wait_recv()
-                twin_copy(owner, kind, slot).start()
+                twin_copy(lax.rem(s + k, sp_size), kind, slot).start()
 
     def take(kind, slot):
         @pl.when(jnp.logical_not(is_owner))
@@ -499,7 +499,7 @@
             q_stage.at[g, aligned(b * pair + core * rows + start, count, ROWS)],
             queries.at[b, aligned(source * rows + start, count, ROWS)],
             q_send.at[2 * g + rel],
-            q_recv.at[source, b],
+            q_recv.at[b],
             sp=base + c * heads + g,
             tp=twin if rel else t,
         )
@@ -510,7 +510,7 @@
             out_stage.at[b, aligned(to * rows, rows, ROWS)],
             attended.at[b, index],
             out_send.at[k],
-            out_recv.at[b, index],
+            out_recv.at[b],
             sp=base + to,
         )
 
@@ -529,8 +529,10 @@
     def process(b, kind, slot, start):
         count = rows if kind == "block" else half_rows
         first_part = start // ROWS
-        for i in range(count // ROWS):
-            token_copy(2, b, 1 - c, first_part + i).wait_recv()
+        for i in range(count // half_rows):
+            place = tokens.at[:half_rows]
+            arrived = twin_recv.at[2 * b + lax.div(first_part, half_parts) + i]
+            remote(place, place, tok_send.at[2, 0], arrived, tp=twin).wait_recv()
         if kind == "block":
             normalise(tokens, lambda g: b * pair + g * half_rows, 4, 0)
         else:
@@ -657,12 +659,12 @@
         return peak, sums, found
 
     def wait_queries(b):
-        for k in range(plane):
-            source = lax.rem(my_head + k, plane)
-
-            @pl.when(jnp.logical_or(k > 0, jnp.logical_not(is_owner)))
-            def _():
-                q_copy(0, 0, source, b, 0, rows).wait_recv()
+        for others in (plane - 1, plane):
+
+            @pl.when(is_owner if others < plane else jnp.logical_not(is_owner))
+            def _():
+                place = queries.at[b, : others * rows]
+                remote(place, place, q_send.at[0], q_recv.at[b], tp=twin).wait_recv()
 
     def begin(b):
         wait_queries(b)
@@ -730,7 +732,7 @@
             stage.at[b, :, cols],
             incoming.at[b + 1, :, cols],
             stage_sem.at[0],
-            left_sem.at[b * UNITS + n],
+            sums_sem.at[(b + 1) * UNITS + n],
             tp=t + 2,
         )
 
@@ -740,7 +742,7 @@
             stage.at[b, :, cols],
             incoming.at[b, :, cols],
             stage_sem.at[0],
-            right_sem.at[b * UNITS + n],
+            sums_sem.at[b * UNITS + n],
             tp=t - 2,
         )
 
@@ -767,7 +769,7 @@
         index, n = lax.div(q, UNITS), lax.rem(q, UNITS)
         n = jnp.where(n == 0, 2, jnp.where(n == 3, 3, n - 1))
         for place, (i, piece_of) in enumerate(
-            [(0, 0), (0, 2), (1, 2), (1, 0), (1, 1), (1, 3), (0, 1), (0, 3)]
+            [(0, 0), (1, 2), (1, 0), (1, 1), (1, 3), (0, 2), (0, 1), (0, 3)]
         ):
             index = jnp.where(q == place, i, index)
             n = jnp.where(q == place, piece_of, n)
@@ -784,8 +786,8 @@
 
     def project(i):
         b = block_of(swap(i))
-        for k in range(1, plane):
-            out_copy(b, k, lax.rem(my_head + k, plane)).wait_recv()
+        place = attended.at[b, : plane - 1]
+        remote(place, place, out_send.at[1], out_recv.at[b], tp=twin).wait_recv()
         sends = at_end & (b != z)
 
         @pl.when(sends)
@@ -900,7 +902,7 @@
     def copies_left():
         for k in range(1, plane):
             remote(
-                attended.at[:, 0], attended.at[:, 0], out_send.at[k], out_recv.at[0, 0], tp=twin
+                attended.at[:, 0], attended.at[:, 0], out_send.at[k], out_recv.at[0], tp=twin
             ).wait_send()
 
         def sent_tokens(b, carry):
@@ -921,18 +923,18 @@
         remote(place, place, tok_send.at[2, 0], tok_recv.at[0], tp=twin).wait_send()
         for g in range(heads):
             place = q_stage.at[g, : chips * rows]
-            remote(place, place, q_send.at[2 * g + 1], q_recv.at[0, 0], tp=twin).wait_send()
+            remote(place, place, q_send.at[2 * g + 1], q_recv.at[0], tp=twin).wait_send()
 
             @pl.when(c * heads + g != my_head)
             def _():
-                remote(place, place, q_send.at[2 * g], q_recv.at[0, 0], tp=twin).wait_send()
+                remote(place, place, q_send.at[2 * g], q_recv.at[0], tp=twin).wait_send()
 
         for k in range(1, sp_size):
 
             @pl.when(wanted(k))
             def _():
                 place = kv_stage.at[0]
-                remote(place, place, kv_send.at[k], kv_recv.at[0, 0], tp=twin).wait_send()
+                remote(place, place, kv_send.at[k], kv_recv.at[0], tp=twin).wait_send()
 
         @pl.when(is_owner)
         def _():
@@ -941,7 +943,7 @@
             ).wait_send()
 
         place = mod_parts.at[: sp_size - 1]
-        remote(place, place, part_send, part_recv.at[0], tp=twin).wait_send()
+        remote(place, place, part_send, part_recv, tp=twin).wait_send()
         place = mod_pieces.at[: tp_size - 1]
         remote(place, place, piece_send, piece_recv.at[0], tp=twin).wait_send()
         head_copy(c).wait_send()
@@ -979,7 +981,7 @@
     @pl.when(at_end)
     def _():
         place = stage.at[: chips - 1, :, :kept]
-        remote(place, place, stage_sem.at[0], left_sem.at[0], tp=twin).wait_send()
+        remote(place, place, stage_sem.at[0], sums_sem.at[0], tp=twin).wait_send()
         lend.wait_send()
         place = attended.at[: chips - 1]
         remote(place, place, lend_send.at[2], block_recv.at[0], tp=twin).wait_send()
@@ -987,7 +989,7 @@
     @pl.when(jnp.logical_not(at_end))
     def _():
         place = stage.at[: chips - 1]
-        remote(place, place, stage_sem.at[0], left_sem.at[0], tp=twin).wait_send()
+        remote(place, place, stage_sem.at[0], sums_sem.at[0], tp=twin).wait_send()
 
     @pl.when(by_end)
     def _():
@@ -1084,24 +1086,24 @@
             pltpu.VMEM((2, plane * rows, LANES), f32),
             dma((15,)),
             dma((3, chips)),
-            dma((parts * tp_size,)),
+            dma((parts * chips,)),
+            dma((2 * chips,)),
             dma(()),
-            dma((sp_size,)),
+            dma(()),
             dma(()),
             dma((tp_size,)),
             dma((sp_size,)),
             dma((1,)),
-            dma((sp_size, chips + 2)),
+            dma((chips + 2,)),
             dma((chips + 2,)),
             dma((2 * heads,)),
-            dma((plane, chips)),
+            dma((chips,)),
             dma((plane,)),
-            dma((chips, plane)),
+            dma((chips,)),
             dma((2,)),
             dma((2,)),
             dma((1,)),
-            dma((UNITS * chips,)),
-            dma((UNITS * chips,)),
+            dma((UNITS * (chips + 1),)),
             dma((3,)),
             dma((2,)),
             dma((chips,)),

time: 90.2 us -> 88.6 us (0.982)
  Pallas kernels: 89.2 us -> 87.1 us
    pallas_call x1, Pallas kernels: 89.2 us -> 87.1 us  [shards(): pl.pallas_call(functools.partial(block_kernel, sp_size, tp_size), out_sha...]
where the time goes in v5:
time: 88.6 us; the launch traced here: 87.9 us
  Pallas kernels  87.1 us (98%)
    pallas_call x1, Pallas kernels, shards(): pl.pallas_call(functools.partial(block_kernel, sp_size, tp_size), out_sha...  87.1 us

profile of v5, /device:TPU:0, one launch (start us, length us, event | category | flops | bytes accessed | tf_op | source)
XLA Modules:
  0.0 87.9 jit_solution(11583685213636795794)
XLA Ops:
  0.0 87.1 %block.1 = bf16[64,4096]{1,0:T(8,128)(2,1)S(1)} custom-call(bf16[64,4096]{1,0:T(8,128)(2,1)} %latent.1, bf16[128,4096]{1,0:T(8,128)(2,1)} %context.1, f32[1,4096]{1,0:T(1,128)} %bitcast.5, f32[1,4096]{1,0:T(1,128)} %bitcast.6, bf16[3,1024,512]{2,1,0:T(8,128)(2,1)} %modulation.1, bf16[4096,512]{1,0:T(8,128)(2,1)} %query_weight.1, ...), custom_call_target="tpu_custom_call" | custom-call | tf_op jit(solution)/shard_map/block/pallas_call | solution.py:1050
  87.1 0.8 copy.15
